TPU v7x, 512 devices: a whole 4x4x16 slice. The times are simulated.
512 devices in a mesh: sp: 16 (over z), fs: 4 (over y), tp: 8 (over x, core).
Axes of the slice: x: 4, y: 4, z: 16, core: 2. Of those that a mesh axis runs over, the one named last changes fastest.
Arguments:
- stream: bfloat16 [4, 4096, 2048], P('fs', 'sp'), may hold values from -6 to 6
- norm_gain: bfloat16 [2048], replicated, may hold values from 0.099609375 to 1.8984375
- query_weight: bfloat16 [2048, 1024], P(None, 'tp'), may hold values from -0.125 to 0.125
- key_weight: bfloat16 [2048, 1024], P(None, 'tp'), may hold values from -0.125 to 0.125
- value_weight: bfloat16 [2048, 1024], P(None, 'tp'), may hold values from -0.125 to 0.125
- filter_input: bfloat16 [2048, 1024], P(None, 'tp'), may hold values from -0.125 to 0.125
- filter_gate: bfloat16 [2048, 1024], P(None, 'tp'), may hold values from -0.125 to 0.125
- score_offset: bfloat16 [4, 4096, 16], P('fs', 'sp', 'tp'), may hold values from -16 to 0
- head_gain: bfloat16 [1024], P('tp'), may hold values from 0.099609375 to 1.8984375
- filter_taps: bfloat16 [31, 1024], P(None, 'tp'), may hold values from -5 to 5
- channel_gain: bfloat16 [1024], P('tp'), may hold values from 0.099609375 to 1.8984375
- channel_shift: bfloat16 [1024], P('tp'), may hold values from -3 to 3
- attend_out: bfloat16 [1024, 2048], P('tp'), may hold values from -0.125 to 0.125
- filter_out: bfloat16 [1024, 2048], P('tp'), may hold values from -0.125 to 0.125
Outputs:
- mixed_out: bfloat16 [4, 4096, 2048], P('fs', ('sp', 'tp'))
- mass_log: float32 [4, 4096, 16], P('fs', 'sp', 'tp')
All inputs are finite; a program needn't handle non-finite values.
Results may differ from a plain program's by a relative error of at most 0.015.
Values may be sent and summed in bfloat16 or wider, within the bound.
A program may use at most 64 MiB of HBM per device.

v0:
```python
import jax
import jax.numpy as jnp
from jax import lax
from jax.sharding import PartitionSpec as P

HEAD_DIM = 64
CONV = 1024


rms_eps = 1e-06
norm_eps = 1e-05
mass_floor = 0.01


def in_one_piece(arrays, axis, dim, along):
    ends, at = ([], 0)
    for a in arrays[:-1]:
        at += a.shape[along]
        ends.append(at)
    both = jnp.concatenate(arrays, axis=along)
    return tuple(jnp.split(lax.all_gather(both, axis, axis=dim, tiled=True), ends, axis=along))


def shifted(value, axis, steps):
    count = lax.axis_size(axis)
    first, last = (max(0, -steps), min(count, count - steps))
    return lax.ppermute(value, axis, [(source, source + steps) for source in range(first, last)])


def split_up(value, dim, devices):
    shape = value.shape
    tiles = value.reshape(*shape[:dim], devices, shape[dim] // devices, *shape[dim + 1 :])
    return jnp.moveaxis(tiles, dim, 0)


def summed_on_arrival(value, axis, dim):
    devices = lax.axis_size(axis)
    tiles = lax.all_to_all(split_up(value, dim, devices), axis, 0, 0, tiled=True)
    return jnp.sum(tiles.astype(jnp.float32), axis=0)


def local(
    stream,
    norm_gain,
    query_weight,
    key_weight,
    value_weight,
    filter_input,
    filter_gate,
    score_offset,
    head_gain,
    filter_taps,
    channel_gain,
    channel_shift,
    attend_out,
    filter_out,
):
    rows_here = stream.shape[1]
    xfloat = stream[0].astype(jnp.float32)
    normed = xfloat * lax.rsqrt(jnp.mean(xfloat * xfloat, axis=-1, keepdims=True) + rms_eps)
    normed = (normed * norm_gain.astype(jnp.float32)).astype(jnp.bfloat16)

    def project(weight):
        return jnp.dot(normed, weight, preferred_element_type=jnp.float32).astype(jnp.bfloat16)

    queries = project(query_weight)
    keys_here = project(key_weight)
    values_here = project(value_weight)
    conv_in = project(filter_input)
    conv_gate = project(filter_gate)
    offsets_here = score_offset[0]
    heads_here = offsets_here.shape[1]
    first_pos = lax.axis_index("sp") * rows_here
    position = first_pos + jnp.arange(rows_here, dtype=jnp.int32)
    qheads = queries.reshape(rows_here, heads_here, HEAD_DIM)

    def absorb(state_now, kblock, vblock, oblock, first_key):
        attended, weight_mass, survive = state_now
        span = kblock.shape[0]
        kblock = kblock.reshape(span, heads_here, HEAD_DIM)
        vblock = vblock.reshape(span, heads_here, HEAD_DIM)
        scores = jnp.einsum(
            "thd,shd->hts", qheads, kblock, preferred_element_type=jnp.float32
        ) * HEAD_DIM ** (-0.5)
        scores = scores + oblock.astype(jnp.float32).T[:, None, :]
        key_pos = first_key + jnp.arange(span, dtype=jnp.int32)
        strict = ((key_pos[None, :] < position[:, None]) & (key_pos[None, :] >= 0))[None]
        losing = jnp.where(strict, jax.nn.log_sigmoid(-scores), 0.0)
        beyond = lax.cumsum(losing, axis=2, reverse=True) - losing + survive[:, :, None]
        weights = jnp.where(strict, jnp.exp(jax.nn.log_sigmoid(scores) + beyond), 0.0)
        weight_mass = weight_mass + jnp.sum(weights, axis=2)
        attended = attended + jnp.einsum(
            "hts,shd->thd", weights.astype(jnp.bfloat16), vblock, preferred_element_type=jnp.float32
        )
        survive = survive + jnp.sum(losing, axis=2)
        return (attended, weight_mass, survive)

    initial = (
        jnp.zeros((rows_here, heads_here, HEAD_DIM), jnp.float32),
        jnp.zeros((heads_here, rows_here), jnp.float32),
        jnp.zeros((heads_here, rows_here), jnp.float32),
    )
    keys_all, values_all, offsets_all = in_one_piece(
        (keys_here, values_here, offsets_here), "sp", 0, 1
    )
    total_keys = keys_all.shape[0]
    key_span = min(512, total_keys)
    needed = (first_pos + rows_here + key_span - 1) // key_span

    def key_block(turn_index, state_now):
        first_key = (needed - 1 - turn_index) * key_span
        kblock = lax.dynamic_slice_in_dim(keys_all, first_key, key_span, 0)
        vblock = lax.dynamic_slice_in_dim(values_all, first_key, key_span, 0)
        oblock = lax.dynamic_slice_in_dim(offsets_all, first_key, key_span, 0)
        return absorb(state_now, kblock, vblock, oblock, first_key)

    attended, weight_mass, survive = lax.fori_loop(0, needed, key_block, initial)
    head_scale = lax.rsqrt(jnp.mean(attended * attended, axis=-1, keepdims=True) + rms_eps)
    heads_flat = attended * head_scale * head_gain.astype(jnp.float32).reshape(heads_here, HEAD_DIM)
    heads_flat = heads_flat.astype(jnp.bfloat16).reshape(rows_here, heads_here * HEAD_DIM)
    mass_log = jnp.log(jnp.maximum(weight_mass.T, mass_floor))
    gated_rows = (
        conv_in.astype(jnp.float32) * jax.nn.sigmoid(conv_gate.astype(jnp.float32))
    ).astype(jnp.bfloat16)
    reach_back = filter_taps.shape[0] - 1
    earlier = shifted(gated_rows[rows_here - reach_back :], "sp", 1)
    extended = jnp.concatenate([earlier, gated_rows], axis=0).astype(jnp.float32)
    tap_values = filter_taps.astype(jnp.float32)
    filtered = jnp.zeros((rows_here, gated_rows.shape[1]), jnp.float32)
    for tap_index in range(reach_back + 1):
        filtered = filtered + extended[tap_index : tap_index + rows_here] * tap_values[tap_index]
    totals, squares = lax.psum(
        (jnp.sum(filtered, axis=-1), jnp.sum(filtered * filtered, axis=-1)), "tp"
    )
    center = totals / CONV
    deviation = filtered - center[:, None]
    spread = jnp.maximum(squares / CONV - center * center, 0.0)
    conv_out = jax.nn.silu(
        deviation * lax.rsqrt(spread[:, None] + norm_eps) * channel_gain.astype(jnp.float32)
        + channel_shift.astype(jnp.float32)
    ).astype(jnp.bfloat16)
    mixed_out = summed_on_arrival(
        (
            jnp.dot(heads_flat, attend_out, preferred_element_type=jnp.float32)
            + jnp.dot(conv_out, filter_out, preferred_element_type=jnp.float32)
        ).astype(jnp.bfloat16),
        "tp",
        0,
    )
    return (mixed_out.astype(jnp.bfloat16)[None], mass_log[None])


def solution(mesh):
    return jax.shard_map(
        local,
        mesh=mesh,
        in_specs=(
            P("fs", "sp", None),
            P(),
            P(None, "tp"),
            P(None, "tp"),
            P(None, "tp"),
            P(None, "tp"),
            P(None, "tp"),
            P("fs", "sp", "tp"),
            P("tp"),
            P(None, "tp"),
            P("tp"),
            P("tp"),
            P("tp", None),
            P("tp", None),
        ),
        out_specs=(P("fs", ("sp", "tp"), None), P("fs", "sp", "tp")),
        check_vma=False,
    )
```

profile of v0, /device:TPU:505, one launch (start us, length us, event | category | flops | bytes accessed | tf_op | source)
XLA Modules:
  0.0 196.5 jit_solution(15662746846097810664)
XLA Ops:
  7.2 0.8 convert_element_type.70
  8.1 1.5 fusion.17
  9.6 2.0 %convolution_convert_fusion.3 = bf16[256,128]{0,1:T(8,128)(2,1)S(1)} fusion(bf16[2048,128]{1,0:T(8,128)(2,1)} %param.20, bf16[1,256,2048]{2,1,0:T(8,128)(2,1)} %param.16, f32[2048]{0:T(1024)S(1)} %convert_element_type.70, f32[256]{0:T(256)S(1)} %add_rsqrt_fusion.2), kind=kOutput, calls=%fused_computation.47 | convolution fusion | flops 136347648 | bytes 1647616 | tf_op jit(solution)/shard_map/dot_general | solution.py:64
  11.6 0.6 convolution_convert_fusion.4
  12.2 0.7 pad_maximum_fusion
  12.9 0.5 fusion.27
  13.5 0.5 fusion.26
  14.1 1.3 collective-permute-start
  15.4 0.6 convolution_convert_fusion.2
  16.1 2.3 %collective-permute-done = bf16[30,128]{1,0:T(8,128)(2,1)S(1)} collective-permute-done((bf16[30,128]{1,0:T(8,128)(2,1)S(1)}, bf16[30,128]{1,0:T(8,128)(2,1)S(1)}, u32[]{:S(2)}, u32[]{:S(2)}) %collective-permute-start) | collective-permute-done | bytes 7712 | tf_op jit(solution)/shard_map/ppermute | solution.py:27
  18.5 0.6 fusion.69
  19.1 13.6 %all-reduce = (f32[256]{0:T(256)S(1)}, f32[256]{0:T(256)S(1)}) all-reduce(f32[256]{0:T(256)S(1)} %get-tuple-element.156, f32[256]{0:T(256)S(1)} %get-tuple-element.155), channel_id=1, replica_groups=mesh['sp'=16,'fs'=4,'tp'=8] {'tp'}, use_global_device_ids=true, to_apply=%region_11.12 | all-reduce | flops 512 | bytes 4096 | tf_op jit(solution)/shard_map/psum | solution.py:132
  32.7 45.2 %all-gather.2.cloned.1.call-done = bf16[4096,258]{0,1:T(8,128)(2,1)} async-done(((bf16[256,258]{0,1:T(8,128)(2,1)}), bf16[4096,258]{0,1:T(8,128)(2,1)}) %all-gather.2.cloned.1.call-update) | async-done | bytes 2113552 | tf_op jit(solution)/shard_map/all_gather | solution.py:21
  77.8 3.1 %fusion.73 = (bf16[4096,128]{0,1:T(8,128)(2,1)}, bf16[4096,128]{0,1:T(8,128)(2,1)}) fusion(bf16[4096,258]{0,1:T(8,128)(2,1)} %all-gather.2.cloned.1.call-done), kind=kLoop, calls=%fused_computation.160 | loop fusion | bytes 4194304 | tf_op jit(solution)/shard_map/split | solution.py:21
  81.0 74.7 %while.17 = (s32[]{:T(128)}, f32[256,2,64]{0,2,1:T(8,128)S(1)}, f32[2,256]{1,0:T(2,128)S(1)}, f32[2,256]{1,0:T(2,128)S(1)}, s32[]{:T(128)}, /*index=5*/s32[]{:T(...) while((s32[]{:T(128)}, f32[256,2,64]{0,2,1:T(8,128)S(1)}, ...), condition=%wide.region_6.7_spmd.clone, body=%wide.region_1.6_spmd.clone.sunk | while | flops 109619464 | bytes 13137135 | solution.py:117
  81.2 1.0 constant_dynamic-slice_fusion.3
  82.4 1.0 fusion.101
  83.4 4.8 %fusion.102 = f32[2,256,4,128]{1,2,3,0:T(4,128)S(1)} fusion(f32[2,256,4,128]{1,3,2,0:T(8,128)S(1)} %bitcast.132), kind=kOutput, calls=%fused_computation.16.clone.1 | output fusion | flops 33292288 | bytes 2097152 | tf_op jit(solution)/shard_map/reduce-window.4
  88.7 1.5 fusion.103
  90.2 0.2 fusion.104
  90.5 1.0 constant_dynamic-slice_fusion.3
  91.7 1.0 fusion.101
  92.7 4.8 %fusion.102 = f32[2,256,4,128]{1,2,3,0:T(4,128)S(1)} fusion(f32[2,256,4,128]{1,3,2,0:T(8,128)S(1)} %bitcast.132), kind=kOutput, calls=%fused_computation.16.clone.1 | output fusion | flops 33292288 | bytes 2097152 | tf_op jit(solution)/shard_map/reduce-window.4
  98.0 1.5 fusion.103
  99.5 0.2 fusion.104
  99.8 1.0 constant_dynamic-slice_fusion.3
  101.1 1.0 fusion.101
  102.0 4.8 %fusion.102 = f32[2,256,4,128]{1,2,3,0:T(4,128)S(1)} fusion(f32[2,256,4,128]{1,3,2,0:T(8,128)S(1)} %bitcast.132), kind=kOutput, calls=%fused_computation.16.clone.1 | output fusion | flops 33292288 | bytes 2097152 | tf_op jit(solution)/shard_map/reduce-window.4
  107.1 0.2 copy.25
  107.3 1.5 fusion.103
  108.8 0.2 fusion.104
  109.1 1.0 constant_dynamic-slice_fusion.3
  110.4 1.0 fusion.101
  111.4 4.8 %fusion.102 = f32[2,256,4,128]{1,2,3,0:T(4,128)S(1)} fusion(f32[2,256,4,128]{1,3,2,0:T(8,128)S(1)} %bitcast.132), kind=kOutput, calls=%fused_computation.16.clone.1 | output fusion | flops 33292288 | bytes 2097152 | tf_op jit(solution)/shard_map/reduce-window.4
  116.4 0.2 copy.25
  116.6 1.5 fusion.103
  118.2 0.2 fusion.104
  118.4 1.0 constant_dynamic-slice_fusion.3
  119.7 1.0 fusion.101
  120.7 4.8 %fusion.102 = f32[2,256,4,128]{1,2,3,0:T(4,128)S(1)} fusion(f32[2,256,4,128]{1,3,2,0:T(8,128)S(1)} %bitcast.132), kind=kOutput, calls=%fused_computation.16.clone.1 | output fusion | flops 33292288 | bytes 2097152 | tf_op jit(solution)/shard_map/reduce-window.4
  125.9 1.5 fusion.103
  127.5 0.2 fusion.104
  127.7 1.0 constant_dynamic-slice_fusion.3
  129.0 1.0 fusion.101
  130.0 4.8 %fusion.102 = f32[2,256,4,128]{1,2,3,0:T(4,128)S(1)} fusion(f32[2,256,4,128]{1,3,2,0:T(8,128)S(1)} %bitcast.132), kind=kOutput, calls=%fused_computation.16.clone.1 | output fusion | flops 33292288 | bytes 2097152 | tf_op jit(solution)/shard_map/reduce-window.4
  135.3 1.5 fusion.103
  136.8 0.2 fusion.104
  137.1 1.0 constant_dynamic-slice_fusion.3
  138.3 1.0 fusion.101
  139.3 4.8 %fusion.102 = f32[2,256,4,128]{1,2,3,0:T(4,128)S(1)} fusion(f32[2,256,4,128]{1,3,2,0:T(8,128)S(1)} %bitcast.132), kind=kOutput, calls=%fused_computation.16.clone.1 | output fusion | flops 33292288 | bytes 2097152 | tf_op jit(solution)/shard_map/reduce-window.4
  144.6 1.5 fusion.103
  146.1 0.2 fusion.104
  146.4 1.0 constant_dynamic-slice_fusion.3
  147.6 1.0 fusion.101
  148.6 4.8 %fusion.102 = f32[2,256,4,128]{1,2,3,0:T(4,128)S(1)} fusion(f32[2,256,4,128]{1,3,2,0:T(8,128)S(1)} %bitcast.132), kind=kOutput, calls=%fused_computation.16.clone.1 | output fusion | flops 33292288 | bytes 2097152 | tf_op jit(solution)/shard_map/reduce-window.4
  153.9 1.5 fusion.103
  155.4 0.2 fusion.104
  155.8 0.5 fusion.74
  156.3 0.4 copy-done.2
  156.7 1.5 fusion.16
  158.2 15.6 %all-to-all-start = ((bf16[8,32,2048]{2,1,0:T(8,128)(2,1)}), bf16[8,32,2048]{2,1,0:T(8,128)(2,1)S(1)}, u32[]{:S(2)}, u32[]{:S(2)}) async-start(bf16[8,32,2048]{2,1,0:T(8,128)(2,1)} %bitcast.36), calls=%async_computation | async-start | bytes 2097152 | tf_op jit(solution)/shard_map/all_to_all | solution.py:38
  173.8 0.6 log_bitcast_fusion
  174.4 14.4 %all-to-all-done = bf16[8,32,2048]{2,1,0:T(8,128)(2,1)S(1)} async-done(((bf16[8,32,2048]{2,1,0:T(8,128)(2,1)}), bf16[8,32,2048]{2,1,0:T(8,128)(2,1)S(1)}, u32[]{:S(2)}, u32[]{:S(2)}) %all-to-all-start) | async-done | bytes 1048608 | tf_op jit(solution)/shard_map/all_to_all | solution.py:38
  188.8 0.8 reduce_sum.74
  (137 shorter events, 5.5 us)
Async XLA Ops:
  7.2 148.7 %copy-start = (bf16[128,2048]{1,0:T(8,128)(2,1)S(1)}, bf16[128,2048]{1,0:T(8,128)(2,1)}, u32[]{:S(2)}) copy-start(bf16[128,2048]{1,0:T(8,128)(2,1)} %param.28) | copy-start | bytes 1572868
  7.2 4.4 %copy-start.1 = (bf16[1,256,2048]{2,1,0:T(8,128)(2,1)S(1)}, bf16[1,256,2048]{2,1,0:T(8,128)(2,1)}, u32[]{:S(2)}) copy-start(bf16[1,256,2048]{2,1,0:T(8,128)(2,1)} %param.16) | copy-start | bytes 3145732
  7.2 4.4 %copy-start.5 = (bf16[2048,128]{1,0:T(8,128)(2,1)S(1)}, bf16[2048,128]{1,0:T(8,128)(2,1)}, u32[]{:S(2)}) copy-start(bf16[2048,128]{1,0:T(8,128)(2,1)} %param.19) | copy-start | bytes 1572868
  7.2 70.6 %all-gather.2.cloned.1.call-start = ((), (), s32[]{:S(2)}) async-start(), calls=%async_computation.1 | async-start | bytes 2297856 | tf_op jit(solution)/shard_map/all_gather | solution.py:21
  9.6 2.6 %copy-start.4 = (bf16[1,256,2]{1,2,0:T(2,128)(2,1)S(1)}, bf16[1,256,2]{1,2,0:T(2,128)(2,1)}, u32[]{:S(2)}) copy-start(bf16[1,256,2]{1,2,0:T(2,128)(2,1)} %param.23) | copy-start | bytes 3076
  9.6 3.3 %copy-start.6 = (bf16[2048,128]{1,0:T(8,128)(2,1)S(1)}, bf16[2048,128]{1,0:T(8,128)(2,1)}, u32[]{:S(2)}) copy-start(bf16[2048,128]{1,0:T(8,128)(2,1)} %param.21) | copy-start | bytes 1572868
  11.6 1.8 copy-start.7
  13.5 1.9 copy-start.3
  13.5 1.9 copy-start.8
  13.5 2.5 %copy-start.9 = (bf16[128]{0:T(256)(128)(2,1)S(1)}, bf16[128]{0:T(256)(128)(2,1)}, u32[]{:S(2)}) copy-start(bf16[128]{0:T(256)(128)(2,1)} %param.24) | copy-start | bytes 772
  13.5 2.6 %copy-start.10 = (bf16[128]{0:T(256)(128)(2,1)S(1)}, bf16[128]{0:T(256)(128)(2,1)}, u32[]{:S(2)}) copy-start(bf16[128]{0:T(256)(128)(2,1)} %param.27) | copy-start | bytes 772
  13.5 2.6 %copy-start.11 = (bf16[128]{0:T(256)(128)(2,1)S(1)}, bf16[128]{0:T(256)(128)(2,1)}, u32[]{:S(2)}) copy-start(bf16[128]{0:T(256)(128)(2,1)} %param.26) | copy-start | bytes 772
  14.1 4.4 %collective-permute-start = (bf16[30,128]{1,0:T(8,128)(2,1)S(1)}, bf16[30,128]{1,0:T(8,128)(2,1)S(1)}, u32[]{:S(2)}, u32[]{:S(2)}) collective-permute-start(bf16[30,128]{1,0:T(8,128)(2,1)S(1)} %slice.266), channel_id=1, source_target_pairs={{0,32},{32,64},{64,96},{96,128},{128,160},{160,192},{192,224},{224... | collective-permute-start | bytes 23048 | tf_op jit(solution)/shard_map/ppermute | solution.py:27
  77.8 3.1 %slice-start = ((bf16[4096,258]{0,1:T(8,128)(2,1)}), bf16[4096,2]{0,1:T(2,128)(2,1)S(1)}, s32[]{:S(2)}) async-start(bf16[4096,258]{0,1:T(8,128)(2,1)} %all-gather.2.cloned.1.call-done), calls=%async_computation.2 | async-start | bytes 32768 | tf_op jit(solution)/shard_map/split | solution.py:21
  155.7 1.0 copy-start.2
  158.2 30.6 %all-to-all-start = ((bf16[8,32,2048]{2,1,0:T(8,128)(2,1)}), bf16[8,32,2048]{2,1,0:T(8,128)(2,1)S(1)}, u32[]{:S(2)}, u32[]{:S(2)}) async-start(bf16[8,32,2048]{2,1,0:T(8,128)(2,1)} %bitcast.36), calls=%async_computation | async-start | bytes 2097152 | tf_op jit(solution)/shard_map/all_to_all | solution.py:38
Sparse Core Ops, SparseCore 0:
  13.1 64.7 all-gather.1
where the time goes:
time: 197 us; the launch traced here: 196 us
  waiting for transfers between devices  61.9 us (31%)
  other arithmetic  59.6 us (30%)
  starting transfers between devices  16.9 us (9%)
  matrix products  15.7 us (8%)
  between operations  14.3 us (7%)
  blocking collectives  13.6 us (7%)
  local copies, waits for them, and re-layouts  13.4 us (7%)
    all_gather x1, waiting for transfers between devices, in_one_piece(): lax.all_gather(both, axis, axis=dim, tiled=True)  45.2 us
    another operation x16, other arithmetic  38.6 us
    all_to_all x1, starting transfers between devices, summed_on_arrival(): lax.all_to_all(split_up(value, dim, devices), axis, 0, 0, tiled=True)  15.6 us
    all_to_all x1, waiting for transfers between devices, summed_on_arrival(): lax.all_to_all(split_up(value, dim, devices), axis, 0, 0, tiled=True)  14.4 us
    psum x1, blocking collectives, local(): lax.psum((jnp.sum(filtered, axis=-1), jnp.sum(filtered * filtered, axis=-...  13.6 us
    reduce_sum x8, other arithmetic, absorb(): weight_mass = weight_mass + jnp.sum(weights, axis=2)  12.3 us
    dynamic_slice x8, local copies, waits for them, and re-layouts, key_block(): kblock = lax.dynamic_slice_in_dim(keys_all, first_key, key_span, 0)  7.94 us
    dot_general x8, matrix products, absorb(): jnp.einsum('thd,shd->hts', qheads, kblock, preferred_element_type=jnp.flo...  7.84 us
  transfers between devices with their start and end apart: 3, of which 3 were waited for; matrix products, arithmetic and copies ran while one was open for 1% of the time, Pallas kernels for 0%

commit v1 on v0

v1 whole, which is shorter than its diff:
```python
import functools

import jax
import jax.numpy as jnp
from jax import lax
from jax.experimental import pallas as pl
from jax.experimental.pallas import tpu as pltpu
from jax.sharding import PartitionSpec as P

HEAD_DIM = 64

rms_eps = 1e-06
norm_eps = 1e-05
mass_floor = 0.01

MESH = pl.DeviceIdType.MESH
f32 = jnp.float32
bf16 = jnp.bfloat16


def dot_nt(a, b):
    return lax.dot_general(a, b, (((1,), (1,)), ((), ())), preferred_element_type=f32)


def kernel(
    n,
    tps,
    x_hbm,
    gain_ref,
    wq_hbm,
    wk_hbm,
    wv_hbm,
    wi_hbm,
    wg_hbm,
    off_ref,
    head_gain_ref,
    taps_ref,
    cgain_ref,
    cshift_ref,
    ao_hbm,
    fo_hbm,
    out_ref,
    mass_ref,
    x_v,
    normed,
    w_v,
    wcat,
    kbuf,
    vbuf,
    obuf,
    qs,
    tri,
    acc_r,
    sum_r,
    acc_l,
    sum_l,
    gated,
    halo,
    ext,
    filt,
    stat_send,
    stat_recv,
    cat,
    part,
    recv,
    load_sem,
    plus_send,
    plus_recv,
    minus_send,
    minus_recv,
    halo_sem,
    stat_ssem,
    stat_rsem,
    rs_ssem,
    rs_rsem,
):
    rows = x_hbm.shape[0]
    width = wq_hbm.shape[1]
    reach = taps_ref.shape[0] - 1
    me = lax.axis_index("sp")
    tp = lax.axis_index("tp")
    right = lax.rem(me + 1, n)
    left = lax.rem(me + n - 1, n)
    dist = n // 2
    low = n - dist - 2

    loads = [
        (x_hbm, x_v),
        (wk_hbm, w_v.at[:, 0:width]),
        (wv_hbm, w_v.at[:, width : 2 * width]),
        (wq_hbm, w_v.at[:, 2 * width : 3 * width]),
        (wi_hbm, w_v.at[:, 3 * width : 4 * width]),
        (wg_hbm, w_v.at[:, 4 * width : 5 * width]),
        (ao_hbm, wcat.at[0:width]),
        (fo_hbm, wcat.at[width : 2 * width]),
    ]
    copies = [
        pltpu.make_async_copy(src, dst, load_sem.at[i]) for i, (src, dst) in enumerate(loads)
    ]
    for copy in copies:
        copy.start()

    barrier = pltpu.get_barrier_semaphore()
    for neighbour in (left, right):
        pl.semaphore_signal(barrier, inc=1, device_id={"sp": neighbour}, device_id_type=MESH)
    for r in range(1, tps):
        pl.semaphore_signal(
            barrier, inc=1, device_id={"tp": lax.rem(tp + r, tps)}, device_id_type=MESH
        )

    half = rows // 2

    def pieces(slot):
        return [
            obuf.at[slot],
            kbuf.at[slot, pl.ds(0, half)],
            kbuf.at[slot, pl.ds(half, half)],
            vbuf.at[slot, pl.ds(0, half)],
            vbuf.at[slot, pl.ds(half, half)],
        ]

    def hop(slot, step, plus):
        ssem, rsem = (plus_send, plus_recv) if plus else (minus_send, minus_recv)
        to = right if plus else left
        return [
            pltpu.make_async_remote_copy(
                src_ref=piece,
                dst_ref=piece,
                send_sem=ssem.at[step, i],
                recv_sem=rsem.at[step, i],
                device_id={"sp": to},
                device_id_type=MESH,
            )
            for i, piece in enumerate(pieces(slot))
        ]

    def plus_sends(step):
        return (me - step >= 0) & (me < n - 1) & (step < dist)

    def minus_gets(device, step):
        block = lax.rem(device + step, n)
        return (step < dist) & (block <= low) & ((device < block) | (device > block + dist))

    def minus_sends(step):
        block = lax.rem(me + step, n)
        fits = (step == 0) | minus_gets(me, step)
        return fits & (block <= low) & minus_gets(left, step + 1)

    row_id = lax.broadcasted_iota(jnp.int32, (rows, rows), 0)
    col_id = lax.broadcasted_iota(jnp.int32, (rows, rows), 1)
    tri[...] = (row_id > col_id).astype(f32).astype(bf16)
    offsets = off_ref[...].astype(f32)
    padded = jnp.concatenate([offsets, jnp.zeros((rows, 126), f32)], axis=1)
    obuf[me] = padded.T[0:2].astype(bf16)

    gain = gain_ref[...].astype(f32).reshape(1, gain_ref.shape[0])
    copies[0].wait()

    @pl.loop(0, rows // 32)
    def _(i):
        at = pl.ds(pl.multiple_of(i * 32, 32), 32)
        xf = x_v[at].astype(f32)
        scale = lax.rsqrt(jnp.mean(xf * xf, axis=-1, keepdims=True) + rms_eps)
        normed[at] = (xf * scale * gain).astype(bf16)

    copies[1].wait()
    copies[2].wait()
    kv = jnp.dot(normed[...], w_v[:, 0 : 2 * width], preferred_element_type=f32)
    kbuf[me] = kv[:, 0:width].astype(bf16)
    vbuf[me] = kv[:, width : 2 * width].astype(bf16)

    pl.semaphore_wait(barrier, tps + 1)

    @pl.when(plus_sends(0))
    def _():
        for copy in hop(me, 0, True):
            copy.start()

    @pl.when(minus_sends(0))
    def _():
        for copy in hop(me, 0, False):
            copy.start()

    for i in (3, 4, 5):
        copies[i].wait()
    qig = jnp.dot(normed[...], w_v[:, 2 * width : 5 * width], preferred_element_type=f32)
    gate = qig[:, 2 * width : 3 * width].astype(bf16).astype(f32)
    conv_in = qig[:, width : 2 * width].astype(bf16).astype(f32)
    gated_rows = (conv_in * (1.0 / (1.0 + jnp.exp(-gate)))).astype(bf16)
    gated[...] = gated_rows
    tail = 32
    halo_copy = pltpu.make_async_remote_copy(
        src_ref=gated.at[pl.ds(rows - tail, tail)],
        dst_ref=halo,
        send_sem=halo_sem.at[0],
        recv_sem=halo_sem.at[1],
        device_id={"sp": right},
        device_id_type=MESH,
    )

    @pl.when(me < n - 1)
    def _():
        halo_copy.start()

    lane = lax.broadcasted_iota(jnp.int32, (rows, width), 1)
    first = lane < HEAD_DIM
    query = qig[:, 0:width].astype(bf16).astype(f32) * HEAD_DIM ** (-0.5)
    qs[0:rows] = jnp.where(first, query, 0.0).astype(bf16)
    qs[rows : 2 * rows] = jnp.where(first, 0.0, query).astype(bf16)

    def attend(slot, chunk, strict):
        head = chunk * half // rows
        at = pl.ds(chunk * half, half)
        scores = dot_nt(qs[at], kbuf[slot]) + obuf[slot].astype(f32)[head : head + 1]
        soft = jnp.maximum(scores, 0.0) + jnp.log(1.0 + jnp.exp(-jnp.abs(scores)))
        gain_log = scores - soft
        if strict is not None:
            soft = jnp.where(strict, soft, 0.0)
        beyond = jnp.dot(soft.astype(bf16), tri[...], preferred_element_type=f32)
        weights = jnp.exp(gain_log - beyond)
        if strict is not None:
            weights = jnp.where(strict, weights, 0.0)
        part_sum = jnp.dot(weights.astype(bf16), vbuf[slot], preferred_element_type=f32)
        lost = jnp.broadcast_to(beyond[:, 0:1] + soft[:, 0:1], (half, width))
        return at, part_sum, lost

    chunks = 2 * rows // half
    for chunk in range(chunks):
        base = chunk * half % rows
        query_pos = lax.broadcasted_iota(jnp.int32, (half, rows), 0) + base
        key_pos = lax.broadcasted_iota(jnp.int32, (half, rows), 1)
        at, part_sum, lost = attend(me, chunk, key_pos < query_pos)
        acc_r[at] = part_sum
        sum_r[at] = lost
    acc_l[...] = jnp.zeros_like(acc_l)
    sum_l[...] = jnp.zeros_like(sum_l)

    stat_copies = [
        pltpu.make_async_remote_copy(
            src_ref=stat_send,
            dst_ref=stat_recv.at[r],
            send_sem=stat_ssem.at[r],
            recv_sem=stat_rsem.at[r],
            device_id={"tp": lax.rem(tp + r, tps)},
            device_id_type=MESH,
        )
        for r in range(1, tps)
    ]

    def convolve():
        @pl.when(me > 0)
        def _():
            halo_copy.wait_recv()
            ext[0:tail] = halo[...].astype(f32)

        @pl.when(me == 0)
        def _():
            ext[0:tail] = jnp.zeros((tail, width), f32)

        ext[tail : tail + rows] = gated[...].astype(f32)
        taps = taps_ref[...].astype(f32)
        for base in range(0, rows, half):
            total = jnp.zeros((half, width), f32)
            for k in range(reach + 1):
                total = total + ext[base + tail - reach + k : base + tail - reach + k + half] * taps[k : k + 1]
            filt[base : base + half] = total
        filtered = filt[...]
        sums = jnp.sum(filtered, axis=-1, keepdims=True)
        squares = jnp.sum(filtered * filtered, axis=-1, keepdims=True)
        both = jnp.where(lane == 0, sums, squares)
        stat_send[...] = both.T[0:8]
        for copy in stat_copies:
            copy.start()

    def normalize():
        total = stat_send[...]
        for r, copy in enumerate(stat_copies):
            copy.wait()
            total = total + stat_recv[r + 1]
        mean = total / (width * tps)
        center = mean[0:1]
        spread = jnp.maximum(mean[1:2] - center * center, 0.0)
        scale = lax.rsqrt(spread + norm_eps)
        line = lax.broadcasted_iota(jnp.int32, (width, rows), 0)
        columns = jnp.where(line == 0, center, scale).T
        hidden = (filt[...] - columns[:, 0:1]) * columns[:, 1:2]
        hidden = hidden * cgain_ref[...].astype(f32).reshape(1, width)
        hidden = hidden + cshift_ref[...].astype(f32).reshape(1, width)
        cat[:, width : 2 * width] = (hidden * (1.0 / (1.0 + jnp.exp(-hidden)))).astype(bf16)

    @pl.loop(1, dist + 1)
    def _(step):
        plus_block = me - step
        minus_block = lax.rem(me + step, n)
        got_plus = plus_block >= 0
        got_minus = minus_gets(me, step)

        @pl.when(got_plus)
        def _():
            arrived = hop(plus_block, step - 1, True)
            onward = hop(plus_block, step, True)
            for copy, ahead in zip(arrived, onward):
                copy.wait_recv()

                @pl.when(plus_sends(step))
                def _():
                    ahead.start()

        @pl.when(got_minus)
        def _():
            arrived = hop(minus_block, step - 1, False)
            onward = hop(minus_block, step, False)
            for copy, ahead in zip(arrived, onward):
                copy.wait_recv()

                @pl.when(minus_sends(step))
                def _():
                    ahead.start()

        @pl.when(got_plus)
        def _():
            for chunk in range(chunks):
                at, part_sum, lost = attend(plus_block, chunk, None)
                seen = sum_r[at]
                acc_r[at] = acc_r[at] + jnp.exp(-seen) * part_sum
                sum_r[at] = seen + lost

        @pl.when(got_minus & (me > minus_block))
        def _():
            for chunk in range(chunks):
                at, part_sum, lost = attend(minus_block, chunk, None)
                acc_l[at] = part_sum + jnp.exp(-lost) * acc_l[at]
                sum_l[at] = sum_l[at] + lost

        @pl.when(step == 1)
        def _():
            convolve()

        @pl.when(step == min(3, dist))
        def _():
            normalize()

    attended = acc_r[...] + jnp.exp(-sum_r[...]) * acc_l[...]
    lost = sum_r[...] + sum_l[...]
    mass = jnp.log(jnp.maximum(1.0 - jnp.exp(-lost), mass_floor))
    mass_ref[:, 0:1] = mass[0:rows, 0:1]
    mass_ref[:, 1:2] = mass[rows : 2 * rows, 0:1]
    attended = jnp.where(first, attended[0:rows], attended[rows : 2 * rows])
    power = attended * attended
    low_mean = jnp.sum(jnp.where(first, power, 0.0), axis=-1, keepdims=True) / HEAD_DIM
    high_mean = jnp.sum(jnp.where(first, 0.0, power), axis=-1, keepdims=True) / HEAD_DIM
    scale = jnp.where(first, lax.rsqrt(low_mean + rms_eps), lax.rsqrt(high_mean + rms_eps))
    heads = attended * scale * head_gain_ref[...].astype(f32).reshape(1, width)
    cat[:, 0:width] = heads.astype(bf16)

    copies[6].wait()
    copies[7].wait()
    features = wcat.shape[1]
    share = rows // tps
    tiles = 4
    span = features // tiles

    def exchange(tile, r):
        peer = lax.rem(tp + r, tps)
        columns = pl.ds(tile * span, span)
        return pltpu.make_async_remote_copy(
            src_ref=part.at[peer, :, columns],
            dst_ref=recv.at[r, :, columns],
            send_sem=rs_ssem.at[tile, r],
            recv_sem=rs_rsem.at[tile, r],
            device_id={"tp": peer},
            device_id_type=MESH,
        )

    for tile in range(tiles):
        columns = slice(tile * span, (tile + 1) * span)
        product = jnp.dot(cat[...], wcat[:, columns], preferred_element_type=f32).astype(bf16)
        part[:, :, columns] = product.reshape(tps, share, span)
        for r in range(1, tps):
            exchange(tile, r).start()
    for tile in range(tiles):
        columns = slice(tile * span, (tile + 1) * span)
        total = part[tp, :, columns].astype(f32)
        for r in range(1, tps):
            exchange(tile, r).wait()
            total = total + recv[r, :, columns].astype(f32)
        out_ref[:, columns] = total.astype(bf16)

    @pl.when(me < n - 1)
    def _():
        halo_copy.wait_send()

    @pl.loop(0, dist)
    def _(step):
        @pl.when(plus_sends(step))
        def _():
            for copy in hop(me - step, step, True):
                copy.wait_send()

        @pl.when(minus_sends(step))
        def _():
            for copy in hop(lax.rem(me + step, n), step, False):
                copy.wait_send()


def local(n, tps, stream, norm_gain, wq, wk, wv, wi, wg, offset, head_gain, taps, cgain, cshift, ao, fo):
    rows, features = stream.shape[1:]
    width = wq.shape[1]
    dist = n // 2
    dma = pltpu.SemaphoreType.DMA
    vmem = pl.BlockSpec(memory_space=pltpu.VMEM)
    anywhere = pl.BlockSpec(memory_space=pl.ANY)
    mixed, mass = pl.pallas_call(
        functools.partial(kernel, n, tps),
        out_shape=(
            jax.ShapeDtypeStruct((rows // tps, features), bf16),
            jax.ShapeDtypeStruct((rows, 2), f32),
        ),
        in_specs=[anywhere, vmem, anywhere, anywhere, anywhere, anywhere, anywhere]
        + [vmem] * 5
        + [anywhere, anywhere],
        out_specs=(vmem, vmem),
        scratch_shapes=[
            pltpu.VMEM((rows, features), bf16),
            pltpu.VMEM((rows, features), bf16),
            pltpu.VMEM((features, 5 * width), bf16),
            pltpu.VMEM((2 * width, features), bf16),
            pltpu.VMEM((n, rows, width), bf16),
            pltpu.VMEM((n, rows, width), bf16),
            pltpu.VMEM((n, 2, rows), bf16),
            pltpu.VMEM((2 * rows, width), bf16),
            pltpu.VMEM((rows, rows), bf16),
            pltpu.VMEM((2 * rows, width), f32),
            pltpu.VMEM((2 * rows, width), f32),
            pltpu.VMEM((2 * rows, width), f32),
            pltpu.VMEM((2 * rows, width), f32),
            pltpu.VMEM((rows, width), bf16),
            pltpu.VMEM((32, width), bf16),
            pltpu.VMEM((rows + 32, width), f32),
            pltpu.VMEM((rows, width), f32),
            pltpu.VMEM((8, rows), f32),
            pltpu.VMEM((tps, 8, rows), f32),
            pltpu.VMEM((rows, 2 * width), bf16),
            pltpu.VMEM((tps, rows // tps, features), bf16),
            pltpu.VMEM((tps, rows // tps, features), bf16),
            dma((8,)),
            dma((dist, 5)),
            dma((dist, 5)),
            dma((dist, 5)),
            dma((dist, 5)),
            dma((2,)),
            dma((tps,)),
            dma((tps,)),
            dma((4, tps)),
            dma((4, tps)),
        ],
        compiler_params=pltpu.CompilerParams(
            collective_id=0, has_side_effects=True, vmem_limit_bytes=48 * 1024 * 1024
        ),
        name="layer",
    )(stream[0], norm_gain, wq, wk, wv, wi, wg, offset[0], head_gain, taps, cgain, cshift, ao, fo)
    return mixed[None], mass[None]


def solution(mesh):
    return jax.shard_map(
        functools.partial(local, mesh.shape["sp"], mesh.shape["tp"]),
        mesh=mesh,
        in_specs=(
            P("fs", "sp", None),
            P(),
            P(None, "tp"),
            P(None, "tp"),
            P(None, "tp"),
            P(None, "tp"),
            P(None, "tp"),
            P("fs", "sp", "tp"),
            P("tp"),
            P(None, "tp"),
            P("tp"),
            P("tp"),
            P("tp", None),
            P("tp", None),
        ),
        out_specs=(P("fs", ("sp", "tp"), None), P("fs", "sp", "tp")),
        check_vma=False,
    )
```

time: 197 us -> 62.6 us (0.32)
  waiting for transfers between devices: 61.9 us -> 0 us
  other arithmetic: 59.6 us -> 0 us
  Pallas kernels: 0 us -> 50.1 us
  starting transfers between devices: 16.9 us -> 0 us
  matrix products: 15.7 us -> 0 us
  between operations: 14.3 us -> 0.68 us
  blocking collectives: 13.6 us -> 0 us
  local copies, waits for them, and re-layouts: 13.4 us -> 11.3 us
    pallas_call x0 -> x1, Pallas kernels: none -> 50.1 us  [local(): pl.pallas_call(functools.partial(kernel, n, tps), out_shape=(jax.ShapeDty...]
    all_gather x1 -> x0, waiting for transfers between devices: 45.2 us -> none  [in_one_piece(): lax.all_gather(both, axis, axis=dim, tiled=True)]
    another operation x24 -> x0, other arithmetic: 40.1 us -> none
    dot_general x23 -> x0, matrix products: 15.7 us -> none  [the longest x8 7.84 us: absorb(): jnp.einsum('thd,shd->hts', qheads, kblock, preferred_element_type=jnp.flo...]
    all_to_all x1 -> x0, starting transfers between devices: 15.6 us -> none  [summed_on_arrival(): lax.all_to_all(split_up(value, dim, devices), axis, 0, 0, tiled=True)]
    reduce_sum x12 -> x0, other arithmetic: 15.2 us -> none  [the longest x8 12.3 us: absorb(): weight_mass = weight_mass + jnp.sum(weights, axis=2)]
    all_to_all x1 -> x0, waiting for transfers between devices: 14.4 us -> none  [summed_on_arrival(): lax.all_to_all(split_up(value, dim, devices), axis, 0, 0, tiled=True)]
    psum x1 -> x0, blocking collectives: 13.6 us -> none  [local(): lax.psum((jnp.sum(filtered, axis=-1), jnp.sum(filtered * filtered, axis=-...]
  transfers between devices with their start and end apart: 3 -> 0, of which waited for: 3 -> 0; matrix products, arithmetic and copies ran while one was open for 1% -> 0% of each run, Pallas kernels for 0% -> 0%
where the time goes in v1:
time: 62.6 us; the launch traced here: 62.1 us
  Pallas kernels  50.1 us (80%)
  local copies, waits for them, and re-layouts  11.3 us (18%)
  between operations  0.68 us (1%)
    pallas_call x1, Pallas kernels, local(): pl.pallas_call(functools.partial(kernel, n, tps), out_shape=(jax.ShapeDty...  50.1 us
    unnamed x31, local copies, waits for them, and re-layouts  11.3 us

profile of v1, /device:TPU:505, one launch (start us, length us, event | category | flops | bytes accessed | tf_op | source)
XLA Modules:
  0.0 62.1 jit_solution(9884761209930167968)
XLA Ops:
  0.6 0.0 copy-start.13
  0.6 0.7 %copy-done.13 = bf16[1,256,2]{1,2,0:T(2,128)(2,1)S(1)} copy-done((bf16[1,256,2]{1,2,0:T(2,128)(2,1)S(1)}, bf16[1,256,2]{1,2,0:T(2,128)(2,1)}, u32[]{:S(2)}) %copy-start.13) | copy-done | bytes 1048
  1.3 0.0 copy-start.8
  1.3 0.0 copy-start.9
  1.3 0.1 copy.16
  1.5 0.0 copy-start.10
  1.5 0.0 copy-start.11
  1.5 0.0 copy-start.12
  1.5 0.5 copy-done.8
  2.0 0.0 copy-done.9
  2.0 0.1 copy-done.10
  2.1 0.0 copy-done.11
  2.1 0.0 copy-done.12
  2.1 0.0 copy-start
  2.2 1.2 %copy-done = bf16[1,256,2048]{2,1,0:T(8,128)(2,1)S(1)} copy-done((bf16[1,256,2048]{2,1,0:T(8,128)(2,1)S(1)}, bf16[1,256,2048]{2,1,0:T(8,128)(2,1)}, u32[]{:S(2)}) %copy-start) | copy-done | bytes 1048600
  3.4 0.0 copy-start.1
  3.4 1.0 %copy-done.1 = bf16[2048,128]{1,0:T(8,128)(2,1)S(1)} copy-done((bf16[2048,128]{1,0:T(8,128)(2,1)S(1)}, bf16[2048,128]{1,0:T(8,128)(2,1)}, u32[]{:S(2)}) %copy-start.1) | copy-done | bytes 524312
  4.4 0.0 copy-start.2
  4.4 1.0 %copy-done.2 = bf16[2048,128]{1,0:T(8,128)(2,1)S(1)} copy-done((bf16[2048,128]{1,0:T(8,128)(2,1)S(1)}, bf16[2048,128]{1,0:T(8,128)(2,1)}, u32[]{:S(2)}) %copy-start.2) | copy-done | bytes 524312
  5.5 0.0 copy-start.3
  5.5 1.0 %copy-done.3 = bf16[2048,128]{1,0:T(8,128)(2,1)S(1)} copy-done((bf16[2048,128]{1,0:T(8,128)(2,1)S(1)}, bf16[2048,128]{1,0:T(8,128)(2,1)}, u32[]{:S(2)}) %copy-start.3) | copy-done | bytes 524312
  6.5 0.0 copy-start.4
  6.5 1.0 %copy-done.4 = bf16[2048,128]{1,0:T(8,128)(2,1)S(1)} copy-done((bf16[2048,128]{1,0:T(8,128)(2,1)S(1)}, bf16[2048,128]{1,0:T(8,128)(2,1)}, u32[]{:S(2)}) %copy-start.4) | copy-done | bytes 524312
  7.5 0.0 copy-start.5
  7.5 1.0 %copy-done.5 = bf16[2048,128]{1,0:T(8,128)(2,1)S(1)} copy-done((bf16[2048,128]{1,0:T(8,128)(2,1)S(1)}, bf16[2048,128]{1,0:T(8,128)(2,1)}, u32[]{:S(2)}) %copy-start.5) | copy-done | bytes 524312
  8.6 0.0 copy-start.6
  8.6 1.0 %copy-done.6 = bf16[128,2048]{1,0:T(8,128)(2,1)S(1)} copy-done((bf16[128,2048]{1,0:T(8,128)(2,1)S(1)}, bf16[128,2048]{1,0:T(8,128)(2,1)}, u32[]{:S(2)}) %copy-start.6) | copy-done | bytes 524312
  9.6 0.0 copy-start.7
  9.6 1.0 %copy-done.7 = bf16[128,2048]{1,0:T(8,128)(2,1)S(1)} copy-done((bf16[128,2048]{1,0:T(8,128)(2,1)S(1)}, bf16[128,2048]{1,0:T(8,128)(2,1)}, u32[]{:S(2)}) %copy-start.7) | copy-done | bytes 524312
  10.7 50.1 %layer.1 = (bf16[32,2048]{1,0:T(8,128)(2,1)S(1)}, f32[256,2]{1,0:T(8,128)S(1)}) custom-call(bf16[256,2048]{1,0:T(8,128)(2,1)S(1)} %bitcast.4, bf16[2048]{0:T(1024)(128)(2,1)S(1)} %copy-done.9, bf16[2048,128]{1,0:T(8,128)(2,1)S(1)} %copy-done.1, bf16[2048,128]{1,0:T(8,128)(2,1)S(1)} %copy-done.2, bf16[2048,128]{1,0:T(8,128)(2,1)S(1)} %copy-done.3, ...), custom_call_target="tpu_custom_call" | custom-call | tf_op jit(solution)/shard_map/layer/pallas_call | solution.py:413
  60.7 0.7 %copy.17 = f32[1,256,2]{1,2,0:T(2,128)} copy(f32[1,256,2]{2,1,0:T(8,128)S(1)} %bitcast.7) | data formatting | bytes 4096
  61.4 0.7 %copy.19 = bf16[1,32,2048]{2,1,0:T(8,128)(2,1)} copy(bf16[1,32,2048]{2,1,0:T(8,128)(2,1)S(1)} %bitcast.6) | data formatting | bytes 262144
Async XLA Ops:
  0.6 0.7 %copy-start.13 = (bf16[1,256,2]{1,2,0:T(2,128)(2,1)S(1)}, bf16[1,256,2]{1,2,0:T(2,128)(2,1)}, u32[]{:S(2)}) copy-start(bf16[1,256,2]{1,2,0:T(2,128)(2,1)} %param.21) | copy-start | bytes 3076
  1.3 0.7 %copy-start.8 = (bf16[31,128]{1,0:T(8,128)(2,1)S(1)}, bf16[31,128]{1,0:T(8,128)(2,1)}, u32[]{:S(2)}) copy-start(bf16[31,128]{1,0:T(8,128)(2,1)} %taps_ref.1) | copy-start | bytes 23812
  1.3 0.7 %copy-start.9 = (bf16[2048]{0:T(1024)(128)(2,1)S(1)}, bf16[2048]{0:T(1024)(128)(2,1)}, u32[]{:S(2)}) copy-start(bf16[2048]{0:T(1024)(128)(2,1)} %gain_ref.1) | copy-start | bytes 12292
  1.5 0.7 %copy-start.10 = (bf16[128]{0:T(256)(128)(2,1)S(1)}, bf16[128]{0:T(256)(128)(2,1)}, u32[]{:S(2)}) copy-start(bf16[128]{0:T(256)(128)(2,1)} %head_gain_ref.1) | copy-start | bytes 772
  1.5 0.7 %copy-start.11 = (bf16[128]{0:T(256)(128)(2,1)S(1)}, bf16[128]{0:T(256)(128)(2,1)}, u32[]{:S(2)}) copy-start(bf16[128]{0:T(256)(128)(2,1)} %cgain_ref.1) | copy-start | bytes 772
  1.5 0.7 %copy-start.12 = (bf16[128]{0:T(256)(128)(2,1)S(1)}, bf16[128]{0:T(256)(128)(2,1)}, u32[]{:S(2)}) copy-start(bf16[128]{0:T(256)(128)(2,1)} %cshift_ref.1) | copy-start | bytes 772
  2.1 1.2 %copy-start = (bf16[1,256,2048]{2,1,0:T(8,128)(2,1)S(1)}, bf16[1,256,2048]{2,1,0:T(8,128)(2,1)}, u32[]{:S(2)}) copy-start(bf16[1,256,2048]{2,1,0:T(8,128)(2,1)} %param.14) | copy-start | bytes 3145732
  3.4 1.0 %copy-start.1 = (bf16[2048,128]{1,0:T(8,128)(2,1)S(1)}, bf16[2048,128]{1,0:T(8,128)(2,1)}, u32[]{:S(2)}) copy-start(bf16[2048,128]{1,0:T(8,128)(2,1)} %wq_hbm.1) | copy-start | bytes 1572868
  4.4 1.0 %copy-start.2 = (bf16[2048,128]{1,0:T(8,128)(2,1)S(1)}, bf16[2048,128]{1,0:T(8,128)(2,1)}, u32[]{:S(2)}) copy-start(bf16[2048,128]{1,0:T(8,128)(2,1)} %wk_hbm.1) | copy-start | bytes 1572868
  5.5 1.0 %copy-start.3 = (bf16[2048,128]{1,0:T(8,128)(2,1)S(1)}, bf16[2048,128]{1,0:T(8,128)(2,1)}, u32[]{:S(2)}) copy-start(bf16[2048,128]{1,0:T(8,128)(2,1)} %wv_hbm.1) | copy-start | bytes 1572868
  6.5 1.0 %copy-start.4 = (bf16[2048,128]{1,0:T(8,128)(2,1)S(1)}, bf16[2048,128]{1,0:T(8,128)(2,1)}, u32[]{:S(2)}) copy-start(bf16[2048,128]{1,0:T(8,128)(2,1)} %wi_hbm.1) | copy-start | bytes 1572868
  7.5 1.0 %copy-start.5 = (bf16[2048,128]{1,0:T(8,128)(2,1)S(1)}, bf16[2048,128]{1,0:T(8,128)(2,1)}, u32[]{:S(2)}) copy-start(bf16[2048,128]{1,0:T(8,128)(2,1)} %wg_hbm.1) | copy-start | bytes 1572868
  8.6 1.0 %copy-start.6 = (bf16[128,2048]{1,0:T(8,128)(2,1)S(1)}, bf16[128,2048]{1,0:T(8,128)(2,1)}, u32[]{:S(2)}) copy-start(bf16[128,2048]{1,0:T(8,128)(2,1)} %ao_hbm.1) | copy-start | bytes 1572868
  9.6 1.0 %copy-start.7 = (bf16[128,2048]{1,0:T(8,128)(2,1)S(1)}, bf16[128,2048]{1,0:T(8,128)(2,1)}, u32[]{:S(2)}) copy-start(bf16[128,2048]{1,0:T(8,128)(2,1)} %fo_hbm.1) | copy-start | bytes 1572868

commit v2 on v1

--- a/solution.py
+++ b/solution.py
@@ -26,22 +26,27 @@
     n,
     tps,
     x_hbm,
-    gain_ref,
+    gain_hbm,
     wq_hbm,
     wk_hbm,
     wv_hbm,
     wi_hbm,
     wg_hbm,
-    off_ref,
-    head_gain_ref,
-    taps_ref,
-    cgain_ref,
-    cshift_ref,
+    off_hbm,
+    head_gain_hbm,
+    taps_hbm,
+    cgain_hbm,
+    cshift_hbm,
     ao_hbm,
     fo_hbm,
     out_ref,
     mass_ref,
     x_v,
+    gain_ref,
+    head_gain_ref,
+    taps_ref,
+    cgain_ref,
+    cshift_ref,
     normed,
     w_v,
     wcat,
@@ -86,6 +91,8 @@
 
     loads = [
         (x_hbm, x_v),
+        (gain_hbm, gain_ref),
+        (off_hbm, obuf.at[me]),
         (wk_hbm, w_v.at[:, 0:width]),
         (wv_hbm, w_v.at[:, width : 2 * width]),
         (wq_hbm, w_v.at[:, 2 * width : 3 * width]),
@@ -93,11 +100,15 @@
         (wg_hbm, w_v.at[:, 4 * width : 5 * width]),
         (ao_hbm, wcat.at[0:width]),
         (fo_hbm, wcat.at[width : 2 * width]),
+        (taps_hbm, taps_ref),
+        (head_gain_hbm, head_gain_ref),
+        (cgain_hbm, cgain_ref),
+        (cshift_hbm, cshift_ref),
     ]
     copies = [
         pltpu.make_async_copy(src, dst, load_sem.at[i]) for i, (src, dst) in enumerate(loads)
     ]
-    for copy in copies:
+    for copy in copies[0:5]:
         copy.start()
 
     barrier = pltpu.get_barrier_semaphore()
@@ -149,12 +160,12 @@
     row_id = lax.broadcasted_iota(jnp.int32, (rows, rows), 0)
     col_id = lax.broadcasted_iota(jnp.int32, (rows, rows), 1)
     tri[...] = (row_id > col_id).astype(f32).astype(bf16)
-    offsets = off_ref[...].astype(f32)
-    padded = jnp.concatenate([offsets, jnp.zeros((rows, 126), f32)], axis=1)
-    obuf[me] = padded.T[0:2].astype(bf16)
-
+
+    copies[1].wait()
     gain = gain_ref[...].astype(f32).reshape(1, gain_ref.shape[0])
     copies[0].wait()
+    for copy in copies[5:]:
+        copy.start()
 
     @pl.loop(0, rows // 32)
     def _(i):
@@ -163,8 +174,8 @@
         scale = lax.rsqrt(jnp.mean(xf * xf, axis=-1, keepdims=True) + rms_eps)
         normed[at] = (xf * scale * gain).astype(bf16)
 
-    copies[1].wait()
-    copies[2].wait()
+    for i in (2, 3, 4):
+        copies[i].wait()
     kv = jnp.dot(normed[...], w_v[:, 0 : 2 * width], preferred_element_type=f32)
     kbuf[me] = kv[:, 0:width].astype(bf16)
     vbuf[me] = kv[:, width : 2 * width].astype(bf16)
@@ -181,7 +192,7 @@
         for copy in hop(me, 0, False):
             copy.start()
 
-    for i in (3, 4, 5):
+    for i in (5, 6, 7):
         copies[i].wait()
     qig = jnp.dot(normed[...], w_v[:, 2 * width : 5 * width], preferred_element_type=f32)
     gate = qig[:, 2 * width : 3 * width].astype(bf16).astype(f32)
@@ -232,6 +243,8 @@
         at, part_sum, lost = attend(me, chunk, key_pos < query_pos)
         acc_r[at] = part_sum
         sum_r[at] = lost
+    for i in (10, 11, 12, 13):
+        copies[i].wait()
     acc_l[...] = jnp.zeros_like(acc_l)
     sum_l[...] = jnp.zeros_like(sum_l)
 
@@ -288,73 +301,6 @@
         hidden = hidden + cshift_ref[...].astype(f32).reshape(1, width)
         cat[:, width : 2 * width] = (hidden * (1.0 / (1.0 + jnp.exp(-hidden)))).astype(bf16)
 
-    @pl.loop(1, dist + 1)
-    def _(step):
-        plus_block = me - step
-        minus_block = lax.rem(me + step, n)
-        got_plus = plus_block >= 0
-        got_minus = minus_gets(me, step)
-
-        @pl.when(got_plus)
-        def _():
-            arrived = hop(plus_block, step - 1, True)
-            onward = hop(plus_block, step, True)
-            for copy, ahead in zip(arrived, onward):
-                copy.wait_recv()
-
-                @pl.when(plus_sends(step))
-                def _():
-                    ahead.start()
-
-        @pl.when(got_minus)
-        def _():
-            arrived = hop(minus_block, step - 1, False)
-            onward = hop(minus_block, step, False)
-            for copy, ahead in zip(arrived, onward):
-                copy.wait_recv()
-
-                @pl.when(minus_sends(step))
-                def _():
-                    ahead.start()
-
-        @pl.when(got_plus)
-        def _():
-            for chunk in range(chunks):
-                at, part_sum, lost = attend(plus_block, chunk, None)
-                seen = sum_r[at]
-                acc_r[at] = acc_r[at] + jnp.exp(-seen) * part_sum
-                sum_r[at] = seen + lost
-
-        @pl.when(got_minus & (me > minus_block))
-        def _():
-            for chunk in range(chunks):
-                at, part_sum, lost = attend(minus_block, chunk, None)
-                acc_l[at] = part_sum + jnp.exp(-lost) * acc_l[at]
-                sum_l[at] = sum_l[at] + lost
-
-        @pl.when(step == 1)
-        def _():
-            convolve()
-
-        @pl.when(step == min(3, dist))
-        def _():
-            normalize()
-
-    attended = acc_r[...] + jnp.exp(-sum_r[...]) * acc_l[...]
-    lost = sum_r[...] + sum_l[...]
-    mass = jnp.log(jnp.maximum(1.0 - jnp.exp(-lost), mass_floor))
-    mass_ref[:, 0:1] = mass[0:rows, 0:1]
-    mass_ref[:, 1:2] = mass[rows : 2 * rows, 0:1]
-    attended = jnp.where(first, attended[0:rows], attended[rows : 2 * rows])
-    power = attended * attended
-    low_mean = jnp.sum(jnp.where(first, power, 0.0), axis=-1, keepdims=True) / HEAD_DIM
-    high_mean = jnp.sum(jnp.where(first, 0.0, power), axis=-1, keepdims=True) / HEAD_DIM
-    scale = jnp.where(first, lax.rsqrt(low_mean + rms_eps), lax.rsqrt(high_mean + rms_eps))
-    heads = attended * scale * head_gain_ref[...].astype(f32).reshape(1, width)
-    cat[:, 0:width] = heads.astype(bf16)
-
-    copies[6].wait()
-    copies[7].wait()
     features = wcat.shape[1]
     share = rows // tps
     tiles = 4
@@ -372,12 +318,91 @@
             device_id_type=MESH,
         )
 
-    for tile in range(tiles):
-        columns = slice(tile * span, (tile + 1) * span)
-        product = jnp.dot(cat[...], wcat[:, columns], preferred_element_type=f32).astype(bf16)
-        part[:, :, columns] = product.reshape(tps, share, span)
-        for r in range(1, tps):
-            exchange(tile, r).start()
+    def finish():
+        attended = acc_r[...] + jnp.exp(-sum_r[...]) * acc_l[...]
+        lost = sum_r[...] + sum_l[...]
+        mass = jnp.log(jnp.maximum(1.0 - jnp.exp(-jnp.where(first, lost[0:rows], lost[rows : 2 * rows])), mass_floor)).T
+        mass_ref[0:1] = mass[0:1]
+        mass_ref[1:2] = mass[HEAD_DIM : HEAD_DIM + 1]
+        attended = jnp.where(first, attended[0:rows], attended[rows : 2 * rows])
+        power = attended * attended
+        low_mean = jnp.sum(jnp.where(first, power, 0.0), axis=-1, keepdims=True) / HEAD_DIM
+        high_mean = jnp.sum(jnp.where(first, 0.0, power), axis=-1, keepdims=True) / HEAD_DIM
+        scale = jnp.where(first, lax.rsqrt(low_mean + rms_eps), lax.rsqrt(high_mean + rms_eps))
+        heads = attended * scale * head_gain_ref[...].astype(f32).reshape(1, width)
+        cat[:, 0:width] = heads.astype(bf16)
+
+        copies[8].wait()
+        copies[9].wait()
+        for tile in range(tiles):
+            columns = slice(tile * span, (tile + 1) * span)
+            product = jnp.dot(cat[...], wcat[:, columns], preferred_element_type=f32).astype(bf16)
+            part[:, :, columns] = product.reshape(tps, share, span)
+            for r in range(1, tps):
+                exchange(tile, r).start()
+
+    @pl.loop(1, dist + 2)
+    def _(step):
+        plus_block = me - step
+        minus_block = lax.rem(me + step, n)
+        got_plus = (plus_block >= 0) & (step <= dist)
+        got_minus = minus_gets(me, step)
+        past_plus = plus_block + 1
+        past_minus = lax.rem(me + step - 1, n)
+        has_plus = (past_plus >= 0) & (step > 1)
+        has_minus = minus_gets(me, step - 1) & (step > 1) & (me > past_minus)
+        plus_arrived = hop(plus_block, step - 1, True)
+        plus_onward = hop(plus_block, step, True)
+        minus_arrived = hop(minus_block, step - 1, False)
+        minus_onward = hop(minus_block, step, False)
+
+        for i in range(chunks + 1):
+
+            @pl.when(got_plus)
+            def _():
+                plus_arrived[i].wait_recv()
+
+            @pl.when(got_plus & plus_sends(step))
+            def _():
+                plus_onward[i].start()
+
+            @pl.when(got_minus)
+            def _():
+                minus_arrived[i].wait_recv()
+
+            @pl.when(got_minus & minus_sends(step))
+            def _():
+                minus_onward[i].start()
+
+            if i == 0:
+                continue
+            chunk = i - 1
+
+            @pl.when(has_plus)
+            def _():
+                at, part_sum, lost = attend(past_plus, chunk, None)
+                seen = sum_r[at]
+                acc_r[at] = acc_r[at] + jnp.exp(-seen) * part_sum
+                sum_r[at] = seen + lost
+
+            @pl.when(has_minus)
+            def _():
+                at, part_sum, lost = attend(past_minus, chunk, None)
+                acc_l[at] = part_sum + jnp.exp(-lost) * acc_l[at]
+                sum_l[at] = sum_l[at] + lost
+
+        @pl.when(step == 1)
+        def _():
+            convolve()
+
+        @pl.when(step == min(3, dist))
+        def _():
+            normalize()
+
+        @pl.when(step == jnp.clip(me + 1, min(3, dist), dist + 1))
+        def _():
+            finish()
+
     for tile in range(tiles):
         columns = slice(tile * span, (tile + 1) * span)
         total = part[tp, :, columns].astype(f32)
@@ -409,19 +434,22 @@
     dist = n // 2
     dma = pltpu.SemaphoreType.DMA
     vmem = pl.BlockSpec(memory_space=pltpu.VMEM)
-    anywhere = pl.BlockSpec(memory_space=pl.ANY)
+    anywhere = pl.BlockSpec(memory_space=pltpu.HBM)
     mixed, mass = pl.pallas_call(
         functools.partial(kernel, n, tps),
         out_shape=(
             jax.ShapeDtypeStruct((rows // tps, features), bf16),
-            jax.ShapeDtypeStruct((rows, 2), f32),
+            jax.ShapeDtypeStruct((2, rows), f32),
         ),
-        in_specs=[anywhere, vmem, anywhere, anywhere, anywhere, anywhere, anywhere]
-        + [vmem] * 5
-        + [anywhere, anywhere],
+        in_specs=[anywhere] * 14,
         out_specs=(vmem, vmem),
         scratch_shapes=[
             pltpu.VMEM((rows, features), bf16),
+            pltpu.VMEM((features,), bf16),
+            pltpu.VMEM((width,), bf16),
+            pltpu.VMEM(taps.shape, bf16),
+            pltpu.VMEM((width,), bf16),
+            pltpu.VMEM((width,), bf16),
             pltpu.VMEM((rows, features), bf16),
             pltpu.VMEM((features, 5 * width), bf16),
             pltpu.VMEM((2 * width, features), bf16),
@@ -443,7 +471,7 @@
             pltpu.VMEM((rows, 2 * width), bf16),
             pltpu.VMEM((tps, rows // tps, features), bf16),
             pltpu.VMEM((tps, rows // tps, features), bf16),
-            dma((8,)),
+            dma((14,)),
             dma((dist, 5)),
             dma((dist, 5)),
             dma((dist, 5)),
@@ -455,11 +483,11 @@
             dma((4, tps)),
         ],
         compiler_params=pltpu.CompilerParams(
-            collective_id=0, has_side_effects=True, vmem_limit_bytes=48 * 1024 * 1024
+            collective_id=0, has_side_effects=True, vmem_limit_bytes=48000000
         ),
         name="layer",
-    )(stream[0], norm_gain, wq, wk, wv, wi, wg, offset[0], head_gain, taps, cgain, cshift, ao, fo)
-    return mixed[None], mass[None]
+    )(*[pltpu.with_memory_space_constraint(a, pltpu.HBM) for a in (stream[0], norm_gain, wq, wk, wv, wi, wg, offset[0].T, head_gain, taps, cgain, cshift, ao, fo)])
+    return mixed[None], mass.T[None]
 
 
 def solution(mesh):

time: 62.6 us -> 57.3 us (0.915)
  local copies, waits for them, and re-layouts: 11.3 us -> 1.24 us
  Pallas kernels: 50.1 us -> 55.3 us
    unnamed x31 -> x2, local copies, waits for them, and re-layouts: 11.3 us -> 1.24 us
    pallas_call x1, Pallas kernels: 50.1 us -> 55.3 us  [local(): pl.pallas_call(functools.partial(kernel, n, tps), out_shape=(jax.ShapeDty...]
where the time goes in v2:
time: 57.3 us; the launch traced here: 57.2 us
  Pallas kernels  55.3 us (97%)
  local copies, waits for them, and re-layouts  1.24 us (2%)
  between operations  0.64 us (1%)
    pallas_call x1, Pallas kernels, local(): pl.pallas_call(functools.partial(kernel, n, tps), out_shape=(jax.ShapeDty...  55.3 us
    unnamed x2, local copies, waits for them, and re-layouts  1.24 us

profile of v2, /device:TPU:505, one launch (start us, length us, event | category | flops | bytes accessed | tf_op | source)
XLA Modules:
  0.0 57.2 jit_solution(7715197406035033757)
XLA Ops:
  0.6 55.3 %layer.1 = (bf16[32,2048]{1,0:T(8,128)(2,1)S(1)}, f32[2,256]{1,0:T(2,128)S(1)}) custom-call(bf16[256,2048]{1,0:T(8,128)(2,1)} %bitcast.10, bf16[2048]{0:T(1024)(128)(2,1)} %gain_hbm.1, bf16[2048,128]{1,0:T(8,128)(2,1)} %wq_hbm.1, bf16[2048,128]{1,0:T(8,128)(2,1)} %wk_hbm.1, bf16[2048,128]{1,0:T(8,128)(2,1)} %wv_hbm.1, bf16[2048,128]{1,0:T(8,128)(2,1)} %wi_hbm.1, ...), custom_call_target="tpu_custom_call" | custom-call | tf_op jit(solution)/shard_map/layer/pallas_call | solution.py:438
  56.0 0.7 %copy.18 = bf16[1,32,2048]{2,1,0:T(8,128)(2,1)} copy(bf16[1,32,2048]{2,1,0:T(8,128)(2,1)S(1)} %bitcast.8) | data formatting | bytes 262144
  56.6 0.6 %copy.19 = f32[1,256,2]{1,2,0:T(2,128)} copy(f32[1,256,2]{1,2,0:T(2,128)S(1)} %bitcast.9) | data formatting | bytes 4096

commit v3 on v2

--- a/solution.py
+++ b/solution.py
@@ -49,7 +49,8 @@
     cshift_ref,
     normed,
     w_v,
-    wcat,
+    wa,
+    fo_v,
     kbuf,
     vbuf,
     obuf,
@@ -65,9 +66,14 @@
     filt,
     stat_send,
     stat_recv,
-    cat,
+    conv_v,
     part,
+    pair,
+    both,
     recv,
+    conv_sum,
+    head_send,
+    head_recv,
     load_sem,
     plus_send,
     plus_recv,
@@ -76,8 +82,13 @@
     halo_sem,
     stat_ssem,
     stat_rsem,
+    pair_sem,
     rs_ssem,
     rs_rsem,
+    gather_ssem,
+    gather_rsem,
+    head_ssem,
+    head_rsem,
 ):
     rows = x_hbm.shape[0]
     width = wq_hbm.shape[1]
@@ -89,6 +100,9 @@
     dist = n // 2
     low = n - dist - 2
 
+    def rows_of(device):
+        return pl.ds(pl.multiple_of(device * width, width), width)
+
     loads = [
         (x_hbm, x_v),
         (gain_hbm, gain_ref),
@@ -98,8 +112,8 @@
         (wq_hbm, w_v.at[:, 2 * width : 3 * width]),
         (wi_hbm, w_v.at[:, 3 * width : 4 * width]),
         (wg_hbm, w_v.at[:, 4 * width : 5 * width]),
-        (ao_hbm, wcat.at[0:width]),
-        (fo_hbm, wcat.at[width : 2 * width]),
+        (ao_hbm, wa.at[rows_of(tp)]),
+        (fo_hbm, fo_v),
         (taps_hbm, taps_ref),
         (head_gain_hbm, head_gain_ref),
         (cgain_hbm, cgain_ref),
@@ -122,13 +136,12 @@
     half = rows // 2
 
     def pieces(slot):
-        return [
-            obuf.at[slot],
-            kbuf.at[slot, pl.ds(0, half)],
-            kbuf.at[slot, pl.ds(half, half)],
-            vbuf.at[slot, pl.ds(0, half)],
-            vbuf.at[slot, pl.ds(half, half)],
-        ]
+        quarters = [pl.ds(i * rows // 4, rows // 4) for i in range(4)]
+        return (
+            [obuf.at[slot]]
+            + [kbuf.at[slot, quarter] for quarter in quarters]
+            + [vbuf.at[slot, quarter] for quarter in quarters]
+        )
 
     def hop(slot, step, plus):
         ssem, rsem = (plus_send, plus_recv) if plus else (minus_send, minus_recv)
@@ -191,6 +204,42 @@
     def _():
         for copy in hop(me, 0, False):
             copy.start()
+
+    chips = tps // 2
+    chip, core = tp // 2, lax.rem(tp, 2)
+    sibling = tp + 1 - 2 * core
+    ahead = 2 * lax.rem(chip + 1, chips) + core
+    behind = 2 * lax.rem(chip + chips - 1, chips) + core
+    across = 2 * lax.rem(chip + 2, chips) + core
+    fold = width // 4
+
+    def spread(i, device, to, start=0, size=width):
+        part_rows = wa.at[pl.ds(pl.multiple_of(device * width + start, fold), size)]
+        return pltpu.make_async_remote_copy(
+            src_ref=part_rows,
+            dst_ref=part_rows,
+            send_sem=gather_ssem.at[i],
+            recv_sem=gather_rsem.at[i],
+            device_id={"tp": to},
+            device_id_type=MESH,
+        )
+
+    def own_part(q):
+        return (
+            spread(q, tp, ahead, q * fold, fold),
+            spread(4 + q, tp, behind, lax.rem(q + 2, 4) * fold, fold),
+        )
+
+    def onward_part(q):
+        return (
+            spread(8 + q, behind, ahead, q * fold, fold),
+            spread(10 + q, ahead, behind, (q + 2) * fold, fold),
+        )
+
+    aside = [spread(12 + i, device, sibling) for i, device in enumerate((tp, behind, ahead, across))]
+    copies[8].wait()
+    for copy in own_part(0):
+        copy.start()
 
     for i in (5, 6, 7):
         copies[i].wait()
@@ -223,7 +272,7 @@
         head = chunk * half // rows
         at = pl.ds(chunk * half, half)
         scores = dot_nt(qs[at], kbuf[slot]) + obuf[slot].astype(f32)[head : head + 1]
-        soft = jnp.maximum(scores, 0.0) + jnp.log(1.0 + jnp.exp(-jnp.abs(scores)))
+        soft = jnp.maximum(jnp.log(1.0 + jnp.exp(jnp.minimum(scores, 80.0))), scores)
         gain_log = scores - soft
         if strict is not None:
             soft = jnp.where(strict, soft, 0.0)
@@ -271,17 +320,20 @@
             ext[0:tail] = jnp.zeros((tail, width), f32)
 
         ext[tail : tail + rows] = gated[...].astype(f32)
+
+    def filter_rows(base):
         taps = taps_ref[...].astype(f32)
-        for base in range(0, rows, half):
-            total = jnp.zeros((half, width), f32)
-            for k in range(reach + 1):
-                total = total + ext[base + tail - reach + k : base + tail - reach + k + half] * taps[k : k + 1]
-            filt[base : base + half] = total
+        total = jnp.zeros((half, width), f32)
+        for k in range(reach + 1):
+            total = total + ext[base + tail - reach + k : base + tail - reach + k + half] * taps[k : k + 1]
+        filt[base : base + half] = total
+
+    def statistics():
         filtered = filt[...]
         sums = jnp.sum(filtered, axis=-1, keepdims=True)
         squares = jnp.sum(filtered * filtered, axis=-1, keepdims=True)
-        both = jnp.where(lane == 0, sums, squares)
-        stat_send[...] = both.T[0:8]
+        packed = jnp.where(lane == 0, sums, squares)
+        stat_send[...] = packed.T[0:8]
         for copy in stat_copies:
             copy.start()
 
@@ -299,22 +351,33 @@
         hidden = (filt[...] - columns[:, 0:1]) * columns[:, 1:2]
         hidden = hidden * cgain_ref[...].astype(f32).reshape(1, width)
         hidden = hidden + cshift_ref[...].astype(f32).reshape(1, width)
-        cat[:, width : 2 * width] = (hidden * (1.0 / (1.0 + jnp.exp(-hidden)))).astype(bf16)
-
-    features = wcat.shape[1]
+        conv_v[...] = (hidden * (1.0 / (1.0 + jnp.exp(-hidden)))).astype(bf16)
+        copies[9].wait()
+
+    features = wa.shape[1]
     share = rows // tps
     tiles = 4
     span = features // tiles
 
-    def exchange(tile, r):
-        peer = lax.rem(tp + r, tps)
+    def swap(tile):
         columns = pl.ds(tile * span, span)
         return pltpu.make_async_remote_copy(
-            src_ref=part.at[peer, :, columns],
+            src_ref=part.at[:, 1 - core, :, columns],
+            dst_ref=pair.at[:, :, columns],
+            send_sem=pair_sem.at[0, tile],
+            recv_sem=pair_sem.at[1, tile],
+            device_id={"tp": sibling},
+            device_id_type=MESH,
+        )
+
+    def exchange(tile, r):
+        columns = pl.ds(tile * span, span)
+        return pltpu.make_async_remote_copy(
+            src_ref=both.at[r, :, columns],
             dst_ref=recv.at[r, :, columns],
             send_sem=rs_ssem.at[tile, r],
             recv_sem=rs_rsem.at[tile, r],
-            device_id={"tp": peer},
+            device_id={"tp": 2 * lax.rem(chip + r, chips) + core},
             device_id_type=MESH,
         )
 
@@ -330,18 +393,75 @@
         high_mean = jnp.sum(jnp.where(first, 0.0, power), axis=-1, keepdims=True) / HEAD_DIM
         scale = jnp.where(first, lax.rsqrt(low_mean + rms_eps), lax.rsqrt(high_mean + rms_eps))
         heads = attended * scale * head_gain_ref[...].astype(f32).reshape(1, width)
-        cat[:, 0:width] = heads.astype(bf16)
-
-        copies[8].wait()
-        copies[9].wait()
-        for tile in range(tiles):
-            columns = slice(tile * span, (tile + 1) * span)
-            product = jnp.dot(cat[...], wcat[:, columns], preferred_element_type=f32).astype(bf16)
-            part[:, :, columns] = product.reshape(tps, share, span)
-            for r in range(1, tps):
+        head_send[...] = heads.astype(bf16).reshape(tps, share, width)
+        for r in range(1, tps):
+            pass_heads(r).start()
+        head_recv[tp] = head_send[tp]
+
+    def pass_heads(r):
+        peer = lax.rem(tp + r, tps)
+        return pltpu.make_async_remote_copy(
+            src_ref=head_send.at[peer],
+            dst_ref=head_recv.at[tp],
+            send_sem=head_ssem.at[r],
+            recv_sem=head_rsem.at[r],
+            device_id={"tp": peer},
+            device_id_type=MESH,
+        )
+
+    def project(tile):
+        columns = slice(tile * span, (tile + 1) * span)
+        product = jnp.dot(conv_v[...], fo_v[:, columns], preferred_element_type=f32).astype(bf16)
+        part[:, :, :, columns] = product.reshape(chips, 2, share, span)
+        swap(tile).start()
+
+    def reduce_pairs(tile):
+        columns = slice(tile * span, (tile + 1) * span)
+        swap(tile).wait()
+        for r in range(chips):
+            to = lax.rem(chip + r, chips)
+            total = part[to, core, :, columns].astype(f32) + pair[to, :, columns].astype(f32)
+            if r == 0:
+                conv_sum[:, columns] = total
+            else:
+                both[r, :, columns] = total.astype(bf16)
                 exchange(tile, r).start()
 
-    @pl.loop(1, dist + 2)
+    def share_own(q):
+        for copy in own_part(q):
+            copy.start()
+
+    def share_onward(q):
+        for copy, ahead_copy in zip(own_part(q), onward_part(q)):
+            copy.wait_recv()
+            ahead_copy.start()
+
+    def share_aside(i):
+        if i > 0:
+            for q in range(2, 4):
+                own_part(q)[i - 1].wait_recv()
+        aside[i].start()
+
+    jobs = {
+        (1, 1): [functools.partial(share_own, 1)],
+        (2, 1): [functools.partial(share_own, 2)],
+        (3, 1): [functools.partial(share_own, 3)],
+        (1, 3): [convolve, functools.partial(filter_rows, 0)],
+        (1, 5): [functools.partial(filter_rows, half)],
+        (1, 7): [statistics],
+        (3, 4): [normalize],
+        (4, 1): [functools.partial(share_onward, 0)],
+        (5, 1): [functools.partial(share_onward, 1)],
+        (6, 0): [functools.partial(share_aside, 0)],
+        (7, 0): [functools.partial(share_aside, 1)],
+        (8, 0): [functools.partial(share_aside, 2)],
+    }
+    for tile in range(tiles):
+        jobs[4, 3 + tile] = jobs.get((4, 3 + tile), []) + [functools.partial(project, tile)]
+        jobs[5, 3 + tile] = jobs.get((5, 3 + tile), []) + [functools.partial(reduce_pairs, tile)]
+    last = max(dist + 1, 9)
+
+    @pl.loop(1, last + 1)
     def _(step):
         plus_block = me - step
         minus_block = lax.rem(me + step, n)
@@ -349,14 +469,14 @@
         got_minus = minus_gets(me, step)
         past_plus = plus_block + 1
         past_minus = lax.rem(me + step - 1, n)
-        has_plus = (past_plus >= 0) & (step > 1)
+        has_plus = (past_plus >= 0) & (step > 1) & (step <= dist + 1)
         has_minus = minus_gets(me, step - 1) & (step > 1) & (me > past_minus)
         plus_arrived = hop(plus_block, step - 1, True)
         plus_onward = hop(plus_block, step, True)
         minus_arrived = hop(minus_block, step - 1, False)
         minus_onward = hop(minus_block, step, False)
 
-        for i in range(chunks + 1):
+        for i in range(9):
 
             @pl.when(got_plus)
             def _():
@@ -374,42 +494,60 @@
             def _():
                 minus_onward[i].start()
 
-            if i == 0:
-                continue
-            chunk = i - 1
-
-            @pl.when(has_plus)
-            def _():
-                at, part_sum, lost = attend(past_plus, chunk, None)
-                seen = sum_r[at]
-                acc_r[at] = acc_r[at] + jnp.exp(-seen) * part_sum
-                sum_r[at] = seen + lost
-
-            @pl.when(has_minus)
-            def _():
-                at, part_sum, lost = attend(past_minus, chunk, None)
-                acc_l[at] = part_sum + jnp.exp(-lost) * acc_l[at]
-                sum_l[at] = sum_l[at] + lost
-
-        @pl.when(step == 1)
-        def _():
-            convolve()
-
-        @pl.when(step == min(3, dist))
-        def _():
-            normalize()
-
-        @pl.when(step == jnp.clip(me + 1, min(3, dist), dist + 1))
-        def _():
-            finish()
-
+            if i == 2:
+
+                @pl.when(has_plus)
+                def _():
+                    for chunk in range(chunks):
+                        at, part_sum, lost = attend(past_plus, chunk, None)
+                        seen = sum_r[at]
+                        acc_r[at] = acc_r[at] + jnp.exp(-seen) * part_sum
+                        sum_r[at] = seen + lost
+
+            if i == 6:
+
+                @pl.when(has_minus)
+                def _():
+                    for chunk in range(chunks):
+                        at, part_sum, lost = attend(past_minus, chunk, None)
+                        acc_l[at] = part_sum + jnp.exp(-lost) * acc_l[at]
+                        sum_l[at] = sum_l[at] + lost
+
+            for at_step, at_piece in jobs:
+                if at_piece == i:
+
+                    @pl.when(step == at_step)
+                    def _():
+                        for job in jobs[at_step, at_piece]:
+                            job()
+
+    finish()
+    for q in range(2):
+        for copy in onward_part(q):
+            copy.wait_recv()
+    aside[3].start()
     for tile in range(tiles):
         columns = slice(tile * span, (tile + 1) * span)
-        total = part[tp, :, columns].astype(f32)
-        for r in range(1, tps):
+        total = conv_sum[:, columns]
+        for r in range(1, chips):
             exchange(tile, r).wait()
             total = total + recv[r, :, columns].astype(f32)
-        out_ref[:, columns] = total.astype(bf16)
+        conv_sum[:, columns] = total
+    for copy in aside:
+        copy.wait()
+    for q in range(4):
+        for copy in own_part(q):
+            copy.wait_send()
+    for q in range(2):
+        for copy in onward_part(q):
+            copy.wait_send()
+    for r in range(1, tps):
+        pass_heads(r).wait()
+    all_heads = jnp.concatenate([head_recv[i] for i in range(tps)], axis=1)
+    for tile in range(tiles):
+        columns = slice(tile * span, (tile + 1) * span)
+        product = jnp.dot(all_heads, wa[:, columns], preferred_element_type=f32)
+        out_ref[:, columns] = (product + conv_sum[:, columns]).astype(bf16)
 
     @pl.when(me < n - 1)
     def _():
@@ -452,7 +590,8 @@
             pltpu.VMEM((width,), bf16),
             pltpu.VMEM((rows, features), bf16),
             pltpu.VMEM((features, 5 * width), bf16),
-            pltpu.VMEM((2 * width, features), bf16),
+            pltpu.VMEM((tps * width, features), bf16),
+            pltpu.VMEM((width, features), bf16),
             pltpu.VMEM((n, rows, width), bf16),
             pltpu.VMEM((n, rows, width), bf16),
             pltpu.VMEM((n, 2, rows), bf16),
@@ -468,19 +607,29 @@
             pltpu.VMEM((rows, width), f32),
             pltpu.VMEM((8, rows), f32),
             pltpu.VMEM((tps, 8, rows), f32),
-            pltpu.VMEM((rows, 2 * width), bf16),
-            pltpu.VMEM((tps, rows // tps, features), bf16),
-            pltpu.VMEM((tps, rows // tps, features), bf16),
+            pltpu.VMEM((rows, width), bf16),
+            pltpu.VMEM((tps // 2, 2, rows // tps, features), bf16),
+            pltpu.VMEM((tps // 2, rows // tps, features), bf16),
+            pltpu.VMEM((tps // 2, rows // tps, features), bf16),
+            pltpu.VMEM((tps // 2, rows // tps, features), bf16),
+            pltpu.VMEM((rows // tps, features), f32),
+            pltpu.VMEM((tps, rows // tps, width), bf16),
+            pltpu.VMEM((tps, rows // tps, width), bf16),
             dma((14,)),
-            dma((dist, 5)),
-            dma((dist, 5)),
-            dma((dist, 5)),
-            dma((dist, 5)),
+            dma((dist, 9)),
+            dma((dist, 9)),
+            dma((dist, 9)),
+            dma((dist, 9)),
             dma((2,)),
             dma((tps,)),
             dma((tps,)),
-            dma((4, tps)),
-            dma((4, tps)),
+            dma((2, 4)),
+            dma((4, tps // 2)),
+            dma((4, tps // 2)),
+            dma((16,)),
+            dma((16,)),
+            dma((tps,)),
+            dma((tps,)),
         ],
         compiler_params=pltpu.CompilerParams(
             collective_id=0, has_side_effects=True, vmem_limit_bytes=48000000

time: 57.3 us -> 47.7 us (0.83)
  the two profiles are of different devices: /device:TPU:505 before, /device:TPU:385 now
where the time goes in v3:
time: 47.7 us; the launch traced here: 47.5 us
  Pallas kernels  45.6 us (96%)
  local copies, waits for them, and re-layouts  1.24 us (3%)
  between operations  0.64 us (1%)
    pallas_call x1, Pallas kernels, local(): pl.pallas_call(functools.partial(kernel, n, tps), out_shape=(jax.ShapeDty...  45.6 us
    unnamed x2, local copies, waits for them, and re-layouts  1.24 us

profile of v3, /device:TPU:385, one launch (start us, length us, event | category | flops | bytes accessed | tf_op | source)
XLA Modules:
  0.0 47.5 jit_solution(7591719112050412141)
XLA Ops:
  0.6 45.6 %layer.1 = (bf16[32,2048]{1,0:T(8,128)(2,1)S(1)}, f32[2,256]{1,0:T(2,128)S(1)}) custom-call(bf16[256,2048]{1,0:T(8,128)(2,1)} %bitcast.10, bf16[2048]{0:T(1024)(128)(2,1)} %gain_hbm.1, bf16[2048,128]{1,0:T(8,128)(2,1)} %wq_hbm.1, bf16[2048,128]{1,0:T(8,128)(2,1)} %wk_hbm.1, bf16[2048,128]{1,0:T(8,128)(2,1)} %wv_hbm.1, bf16[2048,128]{1,0:T(8,128)(2,1)} %wi_hbm.1, ...), custom_call_target="tpu_custom_call" | custom-call | tf_op jit(solution)/shard_map/layer/pallas_call | solution.py:576
  46.3 0.7 %copy.18 = bf16[1,32,2048]{2,1,0:T(8,128)(2,1)} copy(bf16[1,32,2048]{2,1,0:T(8,128)(2,1)S(1)} %bitcast.8) | data formatting | bytes 262144
  46.9 0.6 %copy.19 = f32[1,256,2]{1,2,0:T(2,128)} copy(f32[1,256,2]{1,2,0:T(2,128)S(1)} %bitcast.9) | data formatting | bytes 4096

commit v4 on v3

--- a/solution.py
+++ b/solution.py
@@ -12,6 +12,8 @@
 rms_eps = 1e-06
 norm_eps = 1e-05
 mass_floor = 0.01
+piece_count = 4
+lead = 16
 
 MESH = pl.DeviceIdType.MESH
 f32 = jnp.float32
@@ -51,9 +53,8 @@
     w_v,
     wa,
     fo_v,
-    kbuf,
-    vbuf,
-    obuf,
+    keep,
+    off_v,
     qs,
     tri,
     acc_r,
@@ -80,15 +81,11 @@
     minus_send,
     minus_recv,
     halo_sem,
-    stat_ssem,
-    stat_rsem,
     pair_sem,
     rs_ssem,
     rs_rsem,
-    gather_ssem,
     gather_rsem,
-    head_ssem,
-    head_rsem,
+    side_sem,
 ):
     rows = x_hbm.shape[0]
     width = wq_hbm.shape[1]
@@ -106,7 +103,7 @@
     loads = [
         (x_hbm, x_v),
         (gain_hbm, gain_ref),
-        (off_hbm, obuf.at[me]),
+        (off_hbm, off_v),
         (wk_hbm, w_v.at[:, 0:width]),
         (wv_hbm, w_v.at[:, width : 2 * width]),
         (wq_hbm, w_v.at[:, 2 * width : 3 * width]),
@@ -135,28 +132,29 @@
 
     half = rows // 2
 
-    def pieces(slot):
-        quarters = [pl.ds(i * rows // 4, rows // 4) for i in range(4)]
-        return (
-            [obuf.at[slot]]
-            + [kbuf.at[slot, quarter] for quarter in quarters]
-            + [vbuf.at[slot, quarter] for quarter in quarters]
+    block_rows = lead + 2 * rows
+    bounds = [0] + [lead + i * 2 * rows // piece_count for i in range(1, piece_count + 1)]
+
+    def send_piece(slot, step, plus, start, size, i):
+        piece = keep.at[slot, pl.ds(start, size)]
+        ssem, rsem = (plus_send, plus_recv) if plus else (minus_send, minus_recv)
+        return pltpu.make_async_remote_copy(
+            src_ref=piece,
+            dst_ref=piece,
+            send_sem=ssem.at[step],
+            recv_sem=rsem.at[step, i],
+            device_id={"sp": right if plus else left},
+            device_id_type=MESH,
         )
 
     def hop(slot, step, plus):
-        ssem, rsem = (plus_send, plus_recv) if plus else (minus_send, minus_recv)
-        to = right if plus else left
         return [
-            pltpu.make_async_remote_copy(
-                src_ref=piece,
-                dst_ref=piece,
-                send_sem=ssem.at[step, i],
-                recv_sem=rsem.at[step, i],
-                device_id={"sp": to},
-                device_id_type=MESH,
-            )
-            for i, piece in enumerate(pieces(slot))
+            send_piece(slot, step, plus, bounds[i], bounds[i + 1] - bounds[i], i)
+            for i in range(piece_count)
         ]
+
+    def whole(slot, step, plus):
+        return send_piece(slot, step, plus, 0, block_rows, 0)
 
     def plus_sends(step):
         return (me - step >= 0) & (me < n - 1) & (step < dist)
@@ -190,8 +188,12 @@
     for i in (2, 3, 4):
         copies[i].wait()
     kv = jnp.dot(normed[...], w_v[:, 0 : 2 * width], preferred_element_type=f32)
-    kbuf[me] = kv[:, 0:width].astype(bf16)
-    vbuf[me] = kv[:, width : 2 * width].astype(bf16)
+    keep[me, lead : lead + rows] = kv[:, 0:width].astype(bf16)
+    keep[me, lead + rows : block_rows] = kv[:, width : 2 * width].astype(bf16)
+    offsets = off_v[...].astype(f32)
+    lines = [offsets[h : h + 1, i : i + width] for h in range(2) for i in range(0, rows, width)]
+    lines.append(jnp.zeros((lead - len(lines), width), f32))
+    keep[me, 0:lead] = jnp.concatenate(lines, axis=0).astype(bf16)
 
     pl.semaphore_wait(barrier, tps + 1)
 
@@ -218,7 +220,7 @@
         return pltpu.make_async_remote_copy(
             src_ref=part_rows,
             dst_ref=part_rows,
-            send_sem=gather_ssem.at[i],
+            send_sem=side_sem.at[4],
             recv_sem=gather_rsem.at[i],
             device_id={"tp": to},
             device_id_type=MESH,
@@ -271,7 +273,12 @@
     def attend(slot, chunk, strict):
         head = chunk * half // rows
         at = pl.ds(chunk * half, half)
-        scores = dot_nt(qs[at], kbuf[slot]) + obuf[slot].astype(f32)[head : head + 1]
+        lines = keep[slot, 0:lead].astype(f32)
+        per_head = rows // width
+        offset = jnp.concatenate(
+            [lines[i : i + 1] for i in range(head * per_head, (head + 1) * per_head)], axis=1
+        )
+        scores = dot_nt(qs[at], keep[slot, lead : lead + rows]) + offset
         soft = jnp.maximum(jnp.log(1.0 + jnp.exp(jnp.minimum(scores, 80.0))), scores)
         gain_log = scores - soft
         if strict is not None:
@@ -280,7 +287,7 @@
         weights = jnp.exp(gain_log - beyond)
         if strict is not None:
             weights = jnp.where(strict, weights, 0.0)
-        part_sum = jnp.dot(weights.astype(bf16), vbuf[slot], preferred_element_type=f32)
+        part_sum = jnp.dot(weights.astype(bf16), keep[slot, lead + rows : block_rows], preferred_element_type=f32)
         lost = jnp.broadcast_to(beyond[:, 0:1] + soft[:, 0:1], (half, width))
         return at, part_sum, lost
 
@@ -301,8 +308,8 @@
         pltpu.make_async_remote_copy(
             src_ref=stat_send,
             dst_ref=stat_recv.at[r],
-            send_sem=stat_ssem.at[r],
-            recv_sem=stat_rsem.at[r],
+            send_sem=side_sem.at[0],
+            recv_sem=side_sem.at[1],
             device_id={"tp": lax.rem(tp + r, tps)},
             device_id_type=MESH,
         )
@@ -339,9 +346,16 @@
 
     def normalize():
         total = stat_send[...]
-        for r, copy in enumerate(stat_copies):
-            copy.wait()
-            total = total + stat_recv[r + 1]
+        pltpu.make_async_remote_copy(
+            src_ref=stat_recv.at[pl.ds(1, tps - 1)],
+            dst_ref=stat_recv.at[pl.ds(1, tps - 1)],
+            send_sem=side_sem.at[0],
+            recv_sem=side_sem.at[1],
+            device_id={"tp": sibling},
+            device_id_type=MESH,
+        ).wait()
+        for r in range(1, tps):
+            total = total + stat_recv[r]
         mean = total / (width * tps)
         center = mean[0:1]
         spread = jnp.maximum(mean[1:2] - center * center, 0.0)
@@ -375,8 +389,8 @@
         return pltpu.make_async_remote_copy(
             src_ref=both.at[r, :, columns],
             dst_ref=recv.at[r, :, columns],
-            send_sem=rs_ssem.at[tile, r],
-            recv_sem=rs_rsem.at[tile, r],
+            send_sem=rs_ssem.at[tile],
+            recv_sem=rs_rsem.at[tile],
             device_id={"tp": 2 * lax.rem(chip + r, chips) + core},
             device_id_type=MESH,
         )
@@ -403,8 +417,8 @@
         return pltpu.make_async_remote_copy(
             src_ref=head_send.at[peer],
             dst_ref=head_recv.at[tp],
-            send_sem=head_ssem.at[r],
-            recv_sem=head_rsem.at[r],
+            send_sem=side_sem.at[2],
+            recv_sem=side_sem.at[3],
             device_id={"tp": peer},
             device_id_type=MESH,
         )
@@ -476,23 +490,26 @@
         minus_arrived = hop(minus_block, step - 1, False)
         minus_onward = hop(minus_block, step, False)
 
-        for i in range(9):
-
-            @pl.when(got_plus)
-            def _():
-                plus_arrived[i].wait_recv()
-
-            @pl.when(got_plus & plus_sends(step))
-            def _():
-                plus_onward[i].start()
-
-            @pl.when(got_minus)
-            def _():
-                minus_arrived[i].wait_recv()
-
-            @pl.when(got_minus & minus_sends(step))
-            def _():
-                minus_onward[i].start()
+        for i in range(8):
+            piece, rest = divmod(i * piece_count, 8)
+
+            if rest == 0:
+
+                @pl.when(got_plus)
+                def _():
+                    plus_arrived[piece].wait_recv()
+
+                @pl.when(got_plus & plus_sends(step))
+                def _():
+                    plus_onward[piece].start()
+
+                @pl.when(got_minus)
+                def _():
+                    minus_arrived[piece].wait_recv()
+
+                @pl.when(got_minus & minus_sends(step))
+                def _():
+                    minus_onward[piece].start()
 
             if i == 2:
 
@@ -529,20 +546,28 @@
     for tile in range(tiles):
         columns = slice(tile * span, (tile + 1) * span)
         total = conv_sum[:, columns]
+        pltpu.make_async_remote_copy(
+            src_ref=both.at[pl.ds(1, chips - 1), :, columns],
+            dst_ref=recv.at[pl.ds(1, chips - 1), :, columns],
+            send_sem=rs_ssem.at[tile],
+            recv_sem=rs_rsem.at[tile],
+            device_id={"tp": sibling},
+            device_id_type=MESH,
+        ).wait()
         for r in range(1, chips):
-            exchange(tile, r).wait()
             total = total + recv[r, :, columns].astype(f32)
         conv_sum[:, columns] = total
     for copy in aside:
-        copy.wait()
-    for q in range(4):
-        for copy in own_part(q):
-            copy.wait_send()
-    for q in range(2):
-        for copy in onward_part(q):
-            copy.wait_send()
-    for r in range(1, tps):
-        pass_heads(r).wait()
+        copy.wait_recv()
+    spread(12, 0, sibling, 0, 4 * width + 12 * fold).wait_send()
+    pltpu.make_async_remote_copy(
+        src_ref=head_send.at[pl.ds(1, tps - 1)],
+        dst_ref=head_recv.at[pl.ds(1, tps - 1)],
+        send_sem=side_sem.at[2],
+        recv_sem=side_sem.at[3],
+        device_id={"tp": sibling},
+        device_id_type=MESH,
+    ).wait()
     all_heads = jnp.concatenate([head_recv[i] for i in range(tps)], axis=1)
     for tile in range(tiles):
         columns = slice(tile * span, (tile + 1) * span)
@@ -557,13 +582,11 @@
     def _(step):
         @pl.when(plus_sends(step))
         def _():
-            for copy in hop(me - step, step, True):
-                copy.wait_send()
+            whole(me - step, step, True).wait_send()
 
         @pl.when(minus_sends(step))
         def _():
-            for copy in hop(lax.rem(me + step, n), step, False):
-                copy.wait_send()
+            whole(lax.rem(me + step, n), step, False).wait_send()
 
 
 def local(n, tps, stream, norm_gain, wq, wk, wv, wi, wg, offset, head_gain, taps, cgain, cshift, ao, fo):
@@ -592,9 +615,8 @@
             pltpu.VMEM((features, 5 * width), bf16),
             pltpu.VMEM((tps * width, features), bf16),
             pltpu.VMEM((width, features), bf16),
-            pltpu.VMEM((n, rows, width), bf16),
-            pltpu.VMEM((n, rows, width), bf16),
-            pltpu.VMEM((n, 2, rows), bf16),
+            pltpu.VMEM((n, lead + 2 * rows, width), bf16),
+            pltpu.VMEM((2, rows), bf16),
             pltpu.VMEM((2 * rows, width), bf16),
             pltpu.VMEM((rows, rows), bf16),
             pltpu.VMEM((2 * rows, width), f32),
@@ -616,20 +638,16 @@
             pltpu.VMEM((tps, rows // tps, width), bf16),
             pltpu.VMEM((tps, rows // tps, width), bf16),
             dma((14,)),
-            dma((dist, 9)),
-            dma((dist, 9)),
-            dma((dist, 9)),
-            dma((dist, 9)),
+            dma((dist,)),
+            dma((dist, piece_count)),
+            dma((dist,)),
+            dma((dist, piece_count)),
             dma((2,)),
-            dma((tps,)),
-            dma((tps,)),
             dma((2, 4)),
-            dma((4, tps // 2)),
-            dma((4, tps // 2)),
+            dma((4,)),
+            dma((4,)),
             dma((16,)),
-            dma((16,)),
-            dma((tps,)),
-            dma((tps,)),
+            dma((5,)),
         ],
         compiler_params=pltpu.CompilerParams(
             collective_id=0, has_side_effects=True, vmem_limit_bytes=48000000

time: 47.7 us -> 45.9 us (0.962)
  the two profiles are of different devices: /device:TPU:385 before, /device:TPU:433 now
where the time goes in v4:
time: 45.9 us; the launch traced here: 45.7 us
  Pallas kernels  43.8 us (95%)
  local copies, waits for them, and re-layouts  1.24 us (3%)
  between operations  0.64 us (1%)
    pallas_call x1, Pallas kernels, local(): pl.pallas_call(functools.partial(kernel, n, tps), out_shape=(jax.ShapeDty...  43.8 us
    unnamed x2, local copies, waits for them, and re-layouts  1.24 us

profile of v4, /device:TPU:433, one launch (start us, length us, event | category | flops | bytes accessed | tf_op | source)
XLA Modules:
  0.0 45.7 jit_solution(11586488502161382331)
XLA Ops:
  0.6 43.8 %layer.1 = (bf16[32,2048]{1,0:T(8,128)(2,1)S(1)}, f32[2,256]{1,0:T(2,128)S(1)}) custom-call(bf16[256,2048]{1,0:T(8,128)(2,1)} %bitcast.10, bf16[2048]{0:T(1024)(128)(2,1)} %gain_hbm.1, bf16[2048,128]{1,0:T(8,128)(2,1)} %wq_hbm.1, bf16[2048,128]{1,0:T(8,128)(2,1)} %wk_hbm.1, bf16[2048,128]{1,0:T(8,128)(2,1)} %wv_hbm.1, bf16[2048,128]{1,0:T(8,128)(2,1)} %wi_hbm.1, ...), custom_call_target="tpu_custom_call" | custom-call | tf_op jit(solution)/shard_map/layer/pallas_call | solution.py:599
  44.5 0.7 %copy.18 = bf16[1,32,2048]{2,1,0:T(8,128)(2,1)} copy(bf16[1,32,2048]{2,1,0:T(8,128)(2,1)S(1)} %bitcast.8) | data formatting | bytes 262144
  45.1 0.6 %copy.19 = f32[1,256,2]{1,2,0:T(2,128)} copy(f32[1,256,2]{1,2,0:T(2,128)S(1)} %bitcast.9) | data formatting | bytes 4096

commit v5 on v4

--- a/solution.py
+++ b/solution.py
@@ -271,12 +271,21 @@
     qs[rows : 2 * rows] = jnp.where(first, 0.0, query).astype(bf16)
 
     def attend(slot, chunk, strict):
-        head = chunk * half // rows
-        at = pl.ds(chunk * half, half)
+        at = pl.ds(0, 2 * rows)
         lines = keep[slot, 0:lead].astype(f32)
         per_head = rows // width
         offset = jnp.concatenate(
-            [lines[i : i + 1] for i in range(head * per_head, (head + 1) * per_head)], axis=1
+            [
+                jnp.broadcast_to(
+                    jnp.concatenate(
+                        [lines[head * per_head + i : head * per_head + i + 1] for i in range(per_head)],
+                        axis=1,
+                    ),
+                    (rows, rows),
+                )
+                for head in range(2)
+            ],
+            axis=0,
         )
         scores = dot_nt(qs[at], keep[slot, lead : lead + rows]) + offset
         soft = jnp.maximum(jnp.log(1.0 + jnp.exp(jnp.minimum(scores, 80.0))), scores)
@@ -288,15 +297,12 @@
         if strict is not None:
             weights = jnp.where(strict, weights, 0.0)
         part_sum = jnp.dot(weights.astype(bf16), keep[slot, lead + rows : block_rows], preferred_element_type=f32)
-        lost = jnp.broadcast_to(beyond[:, 0:1] + soft[:, 0:1], (half, width))
+        lost = jnp.broadcast_to(beyond[:, 0:1] + soft[:, 0:1], (2 * rows, width))
         return at, part_sum, lost
 
-    chunks = 2 * rows // half
+    chunks = 1
     for chunk in range(chunks):
-        base = chunk * half % rows
-        query_pos = lax.broadcasted_iota(jnp.int32, (half, rows), 0) + base
-        key_pos = lax.broadcasted_iota(jnp.int32, (half, rows), 1)
-        at, part_sum, lost = attend(me, chunk, key_pos < query_pos)
+        at, part_sum, lost = attend(me, chunk, jnp.concatenate([col_id < row_id] * 2, axis=0))
         acc_r[at] = part_sum
         sum_r[at] = lost
     for i in (10, 11, 12, 13):

time: 45.9 us -> 44.8 us (0.976)
  the two profiles are of different devices: /device:TPU:433 before, /device:TPU:417 now
where the time goes in v5:
time: 44.8 us; the launch traced here: 44.6 us
  Pallas kernels  42.7 us (95%)
  local copies, waits for them, and re-layouts  1.24 us (3%)
  between operations  0.64 us (1%)
    pallas_call x1, Pallas kernels, local(): pl.pallas_call(functools.partial(kernel, n, tps), out_shape=(jax.ShapeDty...  42.7 us
    unnamed x2, local copies, waits for them, and re-layouts  1.24 us

profile of v5, /device:TPU:417, one launch (start us, length us, event | category | flops | bytes accessed | tf_op | source)
XLA Modules:
  0.0 44.6 jit_solution(3648678962122430807)
XLA Ops:
  0.6 42.7 %layer.1 = (bf16[32,2048]{1,0:T(8,128)(2,1)S(1)}, f32[2,256]{1,0:T(2,128)S(1)}) custom-call(bf16[256,2048]{1,0:T(8,128)(2,1)} %bitcast.10, bf16[2048]{0:T(1024)(128)(2,1)} %gain_hbm.1, bf16[2048,128]{1,0:T(8,128)(2,1)} %wq_hbm.1, bf16[2048,128]{1,0:T(8,128)(2,1)} %wk_hbm.1, bf16[2048,128]{1,0:T(8,128)(2,1)} %wv_hbm.1, bf16[2048,128]{1,0:T(8,128)(2,1)} %wi_hbm.1, ...), custom_call_target="tpu_custom_call" | custom-call | tf_op jit(solution)/shard_map/layer/pallas_call | solution.py:605
  43.4 0.7 %copy.18 = bf16[1,32,2048]{2,1,0:T(8,128)(2,1)} copy(bf16[1,32,2048]{2,1,0:T(8,128)(2,1)S(1)} %bitcast.8) | data formatting | bytes 262144
  44.0 0.6 %copy.19 = f32[1,256,2]{1,2,0:T(2,128)} copy(f32[1,256,2]{1,2,0:T(2,128)S(1)} %bitcast.9) | data formatting | bytes 4096

commit v6 on v5

--- a/solution.py
+++ b/solution.py
@@ -97,6 +97,14 @@
     dist = n // 2
     low = n - dist - 2
 
+    barrier = pltpu.get_barrier_semaphore()
+    for neighbour in (left, right):
+        pl.semaphore_signal(barrier, inc=1, device_id={"sp": neighbour}, device_id_type=MESH)
+    for r in range(1, tps):
+        pl.semaphore_signal(
+            barrier, inc=1, device_id={"tp": lax.rem(tp + r, tps)}, device_id_type=MESH
+        )
+
     def rows_of(device):
         return pl.ds(pl.multiple_of(device * width, width), width)
 
@@ -121,14 +129,6 @@
     ]
     for copy in copies[0:5]:
         copy.start()
-
-    barrier = pltpu.get_barrier_semaphore()
-    for neighbour in (left, right):
-        pl.semaphore_signal(barrier, inc=1, device_id={"sp": neighbour}, device_id_type=MESH)
-    for r in range(1, tps):
-        pl.semaphore_signal(
-            barrier, inc=1, device_id={"tp": lax.rem(tp + r, tps)}, device_id_type=MESH
-        )
 
     half = rows // 2
 
@@ -646,8 +646,8 @@
             dma((14,)),
             dma((dist,)),
             dma((dist, piece_count)),
-            dma((dist,)),
-            dma((dist, piece_count)),
+            dma((max(dist - 1, 1),)),
+            dma((max(dist - 1, 1), piece_count)),
             dma((2,)),
             dma((2, 4)),
             dma((4,)),

time: 44.8 us -> 44.8 us (level)
  the two profiles are of different devices: /device:TPU:417 before, /device:TPU:425 now
where the time goes in v6:
time: 44.8 us; the launch traced here: 44.7 us
  Pallas kernels  42.8 us (96%)
  local copies, waits for them, and re-layouts  1.24 us (3%)
  between operations  0.64 us (1%)
    pallas_call x1, Pallas kernels, local(): pl.pallas_call(functools.partial(kernel, n, tps), out_shape=(jax.ShapeDty...  42.8 us
    unnamed x2, local copies, waits for them, and re-layouts  1.24 us

profile of v6, /device:TPU:425, one launch (start us, length us, event | category | flops | bytes accessed | tf_op | source)
XLA Modules:
  0.0 44.7 jit_solution(17916051565723948780)
XLA Ops:
  0.6 42.8 %layer.1 = (bf16[32,2048]{1,0:T(8,128)(2,1)S(1)}, f32[2,256]{1,0:T(2,128)S(1)}) custom-call(bf16[256,2048]{1,0:T(8,128)(2,1)} %bitcast.10, bf16[2048]{0:T(1024)(128)(2,1)} %gain_hbm.1, bf16[2048,128]{1,0:T(8,128)(2,1)} %wq_hbm.1, bf16[2048,128]{1,0:T(8,128)(2,1)} %wk_hbm.1, bf16[2048,128]{1,0:T(8,128)(2,1)} %wv_hbm.1, bf16[2048,128]{1,0:T(8,128)(2,1)} %wi_hbm.1, ...), custom_call_target="tpu_custom_call" | custom-call | tf_op jit(solution)/shard_map/layer/pallas_call | solution.py:605
  43.4 0.7 %copy.18 = bf16[1,32,2048]{2,1,0:T(8,128)(2,1)} copy(bf16[1,32,2048]{2,1,0:T(8,128)(2,1)S(1)} %bitcast.8) | data formatting | bytes 262144
  44.1 0.6 %copy.19 = f32[1,256,2]{1,2,0:T(2,128)} copy(f32[1,256,2]{1,2,0:T(2,128)S(1)} %bitcast.9) | data formatting | bytes 4096
